TPU v7x, 512 devices: a whole 4x4x16 slice. The times are simulated.
512 devices in a mesh: tp: 512 (over z, y, x, core).
Axes of the slice: x: 4, y: 4, z: 16, core: 2. Of those that a mesh axis runs over, the one named last changes fastest.
Arguments:
- stream: bfloat16 [16384, 128], P('tp'), may hold values from -15 to 15
- norm_gain: bfloat16 [4096], replicated, may hold values from 0.099609375 to 1.8984375
- query_weight: bfloat16 [65536, 128], P('tp'), may hold values from -0.09375 to 0.09375
- key_weight: bfloat16 [65536, 128], P('tp'), may hold values from -0.09375 to 0.09375
- value_weight: bfloat16 [65536, 128], P('tp'), may hold values from -0.09375 to 0.09375
- gate_weight: bfloat16 [65536, 128], P('tp'), may hold values from -0.09375 to 0.09375
- write_weight: bfloat16 [4096, 16], replicated, may hold values from -0.09375 to 0.09375
- decay_weight: bfloat16 [4096, 16], replicated, may hold values from -0.09375 to 0.09375
- decay_rate: float32 [16], replicated, may hold values from 0.02 to 2
- head_gain: bfloat16 [128], replicated, may hold values from 0.099609375 to 1.8984375
- out_weight: bfloat16 [65536, 128], P('tp'), may hold values from -0.125 to 0.125
- state: float32 [8192, 128, 128], P('tp'), may hold values from -4 to 4
Outputs:
- stream_out: bfloat16 [16384, 128], P('tp')
- state_out: float32 [8192, 128, 128], P('tp')
All inputs are finite; a program needn't handle non-finite values.
Results may differ from a plain program's by a relative error of at most 0.012.
Values may be sent and summed in bfloat16 or wider, within the bound.
No kernel may reach another device: no remote copies, remote signals or barrier semaphores. Data moves between devices by JAX's collectives and lax.ppermute only.
A program may use at most 64 MiB of HBM per device.

v0:
```python
import jax
import jax.numpy as jnp
from jax import lax
from jax.sharding import PartitionSpec as P

EPS = 1e-06


def from_partner(shard, axis, bit):
    return lax.ppermute(shard, axis, [(i, i ^ 1 << bit) for i in range(lax.axis_size(axis))])


def shortened(shard):

    def short(part):
        return part.astype(jnp.bfloat16) if part.dtype == jnp.float32 else part

    return jax.tree.map(short, shard)


def per_device(
    stream,
    norm_gain,
    query_weight,
    key_weight,
    value_weight,
    gate_weight,
    write_weight,
    decay_weight,
    decay_rate,
    head_gain,
    out_weight,
    state,
):
    devices = lax.axis_size("tp")
    my_index = lax.axis_index("tp")
    head_count = decay_rate.shape[0]
    head_size = head_gain.shape[0]
    group_count = devices // head_count
    head_bits = head_count.bit_length() - 1
    group_bits = group_count.bit_length() - 1
    my_head = my_index % head_count
    my_group = my_index // head_count
    own_rows, own_cols = stream.shape
    model_width = own_cols * group_count
    gathered = stream
    for bit_level in range(head_bits):
        partner = from_partner(gathered, "tp", bit_level)
        upper_bit = my_index // (1 << bit_level) % 2
        gathered = jnp.where(
            upper_bit == 1,
            jnp.concatenate([partner, gathered], 0),
            jnp.concatenate([gathered, partner], 0),
        )
    stream_f = gathered.astype(jnp.float32)
    gain_block = lax.dynamic_slice_in_dim(norm_gain, my_group * own_cols, own_cols, 0).astype(
        jnp.float32
    )
    gained = (stream_f * gain_block[None, :]).astype(jnp.bfloat16)
    squares = jnp.sum(stream_f * stream_f, axis=1)
    write_rows = lax.dynamic_slice(write_weight, (my_group * own_cols, my_head), (own_cols, 1))
    decay_rows = lax.dynamic_slice(decay_weight, (my_group * own_cols, my_head), (own_cols, 1))
    big_weights = jnp.concatenate([query_weight, key_weight, value_weight, gate_weight], axis=1)
    partial_value = jnp.dot(gained, big_weights, preferred_element_type=jnp.float32)
    small_part = jnp.dot(
        gained,
        jnp.concatenate([write_rows, decay_rows], axis=1),
        preferred_element_type=jnp.float32,
    )
    for step_index in range(group_bits):
        bit_level = head_bits + group_bits - 1 - step_index
        upper_bit = my_index // (1 << bit_level) % 2
        half_rows = partial_value.shape[0] // 2
        kept = [
            lax.dynamic_slice_in_dim(member, upper_bit * half_rows, half_rows, 0)
            for member in (partial_value, small_part, squares)
        ]
        sent = [
            lax.dynamic_slice_in_dim(member, (1 - upper_bit) * half_rows, half_rows, 0)
            for member in (partial_value, small_part, squares)
        ]
        received = from_partner(
            (shortened(sent[0]), shortened(sent[1]), shortened(sent[2])), "tp", bit_level
        )
        partial_value = kept[0] + received[0]
        small_part = kept[1] + received[1]
        squares = kept[2] + received[2]
    row_scale = lax.rsqrt(squares / model_width + EPS)
    projected = (partial_value * row_scale[:, None]).astype(jnp.bfloat16).astype(jnp.float32)
    small_pre = (small_part * row_scale[:, None]).astype(jnp.bfloat16).astype(jnp.float32)
    query_raw = projected[:, :head_size]
    key_raw = projected[:, head_size : 2 * head_size]
    value_vec = projected[:, 2 * head_size : 3 * head_size]
    gate_vec = projected[:, 3 * head_size :]
    query_vec = (
        query_raw
        * lax.rsqrt(jnp.sum(query_raw * query_raw, axis=-1, keepdims=True) + EPS)
        * head_size ** (-0.5)
    )
    key_vec = key_raw * lax.rsqrt(jnp.sum(key_raw * key_raw, axis=-1, keepdims=True) + EPS)
    strength = jax.nn.sigmoid(small_pre[:, 0])
    rate_value = lax.dynamic_slice_in_dim(decay_rate, my_head, 1, 0)[0]
    decay_factor = jnp.exp(-rate_value * jax.nn.softplus(small_pre[:, 1]))
    recalled = jnp.einsum("bdj,bd->bj", state, key_vec)
    correction = strength[:, None] * (value_vec - decay_factor[:, None] * recalled)
    updated = decay_factor[:, None, None] * state + key_vec[:, :, None] * correction[:, None, :]
    readout = jnp.einsum("bdj,bd->bj", updated, query_vec)
    scaling = lax.rsqrt(jnp.mean(readout * readout, axis=1) + EPS)
    gated = (readout * head_gain.astype(jnp.float32)[None, :] * jax.nn.silu(gate_vec)).astype(
        jnp.bfloat16
    )
    all_gated = gated
    all_scaling = scaling
    for step_index in range(group_bits):
        bit_level = head_bits + step_index
        upper_bit = my_index // (1 << bit_level) % 2
        other_gated, other_scaling = (
            from_partner(all_gated, "tp", bit_level),
            from_partner(all_scaling.astype(jnp.bfloat16), "tp", bit_level).astype(
                all_scaling.dtype
            ),
        )
        all_gated = jnp.where(
            upper_bit == 1,
            jnp.concatenate([other_gated, all_gated], 0),
            jnp.concatenate([all_gated, other_gated], 0),
        )
        all_scaling = jnp.where(
            upper_bit == 1,
            jnp.concatenate([other_scaling, all_scaling], 0),
            jnp.concatenate([all_scaling, other_scaling], 0),
        )
    head_sums = (
        lax.dot_general(
            all_gated, out_weight, (((1,), (1,)), ((), ())), preferred_element_type=jnp.float32
        )
        * all_scaling[:, None]
    )
    for step_index in range(head_bits):
        bit_level = head_bits - 1 - step_index
        upper_bit = my_index // (1 << bit_level) % 2
        half_rows = head_sums.shape[0] // 2
        kept_sums = lax.dynamic_slice_in_dim(head_sums, upper_bit * half_rows, half_rows, 0)
        sent_sums = lax.dynamic_slice_in_dim(head_sums, (1 - upper_bit) * half_rows, half_rows, 0)
        head_sums = kept_sums + from_partner(
            sent_sums.astype(jnp.bfloat16), "tp", bit_level
        ).astype(sent_sums.dtype)
    result = (stream.astype(jnp.float32) + head_sums).astype(jnp.bfloat16)
    return (result, updated)


def solution(mesh):
    placed = (
        P("tp", None),
        P(),
        P("tp", None),
        P("tp", None),
        P("tp", None),
        P("tp", None),
        P(),
        P(),
        P(),
        P(),
        P("tp", None),
        P("tp", None, None),
    )
    return jax.shard_map(
        per_device,
        mesh=mesh,
        in_specs=placed,
        out_specs=(P("tp", None), P("tp", None, None)),
        check_vma=False,
    )
```

profile of v0, /device:TPU:1, one launch (start us, length us, event | category | flops | bytes accessed | tf_op | source)
XLA Modules:
  0.0 232.1 jit_solution(12539227957241368107)
XLA Ops:
  0.6 8.7 %collective-permute-start = (bf16[32,128]{1,0:T(8,128)(2,1)}, bf16[32,128]{1,0:T(8,128)(2,1)S(1)}, u32[]{:S(2)}, u32[]{:S(2)}) collective-permute-start(bf16[32,128]{1,0:T(8,128)(2,1)} %param.12), channel_id=1, source_target_pairs={{0,1},{1,0},{2,3},{3,2},{4,5},{5,4},{6,7},{7,6},{8,9},{9,8},{10,11... | collective-permute-start | bytes 24584 | tf_op jit(solution)/shard_map/ppermute | solution.py:10
  26.4 11.8 %collective-permute-start.9 = (bf16[256]{0:T(256)(128)(2,1)S(1)}, bf16[256]{0:T(256)(128)(2,1)S(1)}, u32[]{:S(2)}, u32[]{:S(2)}) collective-permute-start(bf16[256]{0:T(256)(128)(2,1)S(1)} %dynamic_slice.235), channel_id=1, source_target_pairs={{0,256},{1,257},{2,258},{3,259},{4,260},{5,261},{6,262},{7,263},{8... | collective-permute-start | bytes 1544 | tf_op jit(solution)/shard_map/ppermute | solution.py:10
  40.8 5.1 %collective-permute-start.10 = (bf16[128]{0:T(256)(128)(2,1)S(1)}, bf16[128]{0:T(256)(128)(2,1)S(1)}, u32[]{:S(2)}, u32[]{:S(2)}) collective-permute-start(bf16[128]{0:T(256)(128)(2,1)S(1)} %dynamic_slice.239), channel_id=1, source_target_pairs={{0,128},{1,129},{2,130},{3,131},{4,132},{5,133},{6,134},{7,135},{8... | collective-permute-start | bytes 776 | tf_op jit(solution)/shard_map/ppermute | solution.py:10
  52.0 12.1 %collective-permute-start.14 = (bf16[256,512]{1,0:T(8,128)(2,1)S(1)}, bf16[256,512]{1,0:T(8,128)(2,1)S(1)}, u32[]{:S(2)}, u32[]{:S(2)}) collective-permute-start(bf16[256,512]{1,0:T(8,128)(2,1)S(1)} %dynamic-slice_convert_fusion), channel_id=1, source_target_pairs={{0,256},{1,257},{2,258},{3,259},{4,260},{5,261},{6,262},{7,263},{8... | collective-permute-start | bytes 786440 | tf_op jit(solution)/shard_map/ppermute | solution.py:10
  66.9 4.0 %collective-permute-start.5 = (bf16[128,2]{0,1:T(2,128)(2,1)S(1)}, bf16[128,2]{0,1:T(2,128)(2,1)S(1)}, u32[]{:S(2)}, u32[]{:S(2)}) collective-permute-start(bf16[128,2]{0,1:T(2,128)(2,1)S(1)} %fusion.24), channel_id=1, source_target_pairs={{0,128},{1,129},{2,130},{3,131},{4,132},{5,133},{6,134},{7,135},{8... | collective-permute-start | bytes 1544 | tf_op jit(solution)/shard_map/ppermute | solution.py:10
  70.9 5.6 %collective-permute-done.12 = bf16[32]{0:T(256)(128)(2,1)S(1)} collective-permute-done((bf16[32]{0:T(256)(128)(2,1)S(1)}, bf16[32]{0:T(256)(128)(2,1)S(1)}, u32[]{:S(2)}, u32[]{:S(2)}) %collective-permute-start.12) | collective-permute-done | bytes 96 | tf_op jit(solution)/shard_map/ppermute | solution.py:10
  76.6 4.8 %collective-permute-start.13 = (bf16[16]{0:T(256)(128)(2,1)S(1)}, bf16[16]{0:T(256)(128)(2,1)S(1)}, u32[]{:S(2)}, u32[]{:S(2)}) collective-permute-start(bf16[16]{0:T(256)(128)(2,1)S(1)} %dynamic_slice.236), channel_id=1, source_target_pairs={{0,16},{1,17},{2,18},{3,19},{4,20},{5,21},{6,22},{7,23},{8,24},{9,... | collective-permute-start | bytes 104 | tf_op jit(solution)/shard_map/ppermute | solution.py:10
  81.6 3.1 %collective-permute-start.6 = (bf16[64,2]{0,1:T(2,128)(2,1)S(1)}, bf16[64,2]{0,1:T(2,128)(2,1)S(1)}, u32[]{:S(2)}, u32[]{:S(2)}) collective-permute-start(bf16[64,2]{0,1:T(2,128)(2,1)S(1)} %fusion.26), channel_id=1, source_target_pairs={{0,64},{1,65},{2,66},{3,67},{4,68},{5,69},{6,70},{7,71},{8,72},{9,... | collective-permute-start | bytes 776 | tf_op jit(solution)/shard_map/ppermute | solution.py:10
  87.0 9.5 %collective-permute-start.7 = (bf16[32,2]{0,1:T(2,128)(2,1)S(1)}, bf16[32,2]{0,1:T(2,128)(2,1)S(1)}, u32[]{:S(2)}, u32[]{:S(2)}) collective-permute-start(bf16[32,2]{0,1:T(2,128)(2,1)S(1)} %fusion.28), channel_id=1, source_target_pairs={{0,32},{1,33},{2,34},{3,35},{4,36},{5,37},{6,38},{7,39},{8,40},{9,... | collective-permute-start | bytes 392 | tf_op jit(solution)/shard_map/ppermute | solution.py:10
  96.6 7.2 %collective-permute-start.15 = (bf16[128,512]{1,0:T(8,128)(2,1)S(1)}, bf16[128,512]{1,0:T(8,128)(2,1)S(1)}, u32[]{:S(2)}, u32[]{:S(2)}) collective-permute-start(bf16[128,512]{1,0:T(8,128)(2,1)S(1)} %dynamic-slice_convert_fusion.1), channel_id=1, source_target_pairs={{0,128},{1,129},{2,130},{3,131},{4,132},{5,133},{6,134},{7,135},{8... | collective-permute-start | bytes 393224 | tf_op jit(solution)/shard_map/ppermute | solution.py:10
  106.0 4.3 %collective-permute-done.15 = bf16[128,512]{1,0:T(8,128)(2,1)S(1)} collective-permute-done((bf16[128,512]{1,0:T(8,128)(2,1)S(1)}, bf16[128,512]{1,0:T(8,128)(2,1)S(1)}, u32[]{:S(2)}, u32[]{:S(2)}) %collective-permute-start.15) | collective-permute-done | bytes 131104 | tf_op jit(solution)/shard_map/ppermute | solution.py:10
  112.4 4.8 %collective-permute-done.16 = bf16[64,512]{1,0:T(8,128)(2,1)S(1)} collective-permute-done((bf16[64,512]{1,0:T(8,128)(2,1)S(1)}, bf16[64,512]{1,0:T(8,128)(2,1)S(1)}, u32[]{:S(2)}, u32[]{:S(2)}) %collective-permute-start.16) | collective-permute-done | bytes 65568 | tf_op jit(solution)/shard_map/ppermute | solution.py:10
  117.2 4.3 %collective-permute-start.17 = (bf16[32,512]{1,0:T(8,128)(2,1)S(1)}, bf16[32,512]{1,0:T(8,128)(2,1)S(1)}, u32[]{:S(2)}, u32[]{:S(2)}) collective-permute-start(bf16[32,512]{1,0:T(8,128)(2,1)S(1)} %dynamic-slice_convert_fusion.5), channel_id=1, source_target_pairs={{0,32},{1,33},{2,34},{3,35},{4,36},{5,37},{6,38},{7,39},{8,40},{9,... | collective-permute-start | bytes 98312 | tf_op jit(solution)/shard_map/ppermute | solution.py:10
  122.9 8.5 %collective-permute-start.18 = (bf16[16,512]{1,0:T(8,128)(2,1)S(1)}, bf16[16,512]{1,0:T(8,128)(2,1)S(1)}, u32[]{:S(2)}, u32[]{:S(2)}) collective-permute-start(bf16[16,512]{1,0:T(8,128)(2,1)S(1)} %dynamic-slice_convert_fusion.7), channel_id=1, source_target_pairs={{0,16},{1,17},{2,18},{3,19},{4,20},{5,21},{6,22},{7,23},{8,24},{9,... | collective-permute-start | bytes 49160 | tf_op jit(solution)/shard_map/ppermute | solution.py:10
  133.9 4.9 %collective-permute-start.24 = (bf16[16]{0:T(256)(128)(2,1)S(1)}, bf16[16]{0:T(256)(128)(2,1)S(1)}, u32[]{:S(2)}, u32[]{:S(2)}) collective-permute-start(bf16[16]{0:T(256)(128)(2,1)S(1)} %get-tuple-element.19), channel_id=1, source_target_pairs={{0,16},{1,17},{2,18},{3,19},{4,20},{5,21},{6,22},{7,23},{8,24},{9,... | collective-permute-start | bytes 104 | tf_op jit(solution)/shard_map/ppermute | solution.py:10
  154.7 8.3 %collective-permute-start.27 = (bf16[128]{0:T(256)(128)(2,1)S(1)}, bf16[128]{0:T(256)(128)(2,1)S(1)}, u32[]{:S(2)}, u32[]{:S(2)}) collective-permute-start(bf16[128]{0:T(256)(128)(2,1)S(1)} %get-tuple-element.6), channel_id=1, source_target_pairs={{0,128},{1,129},{2,130},{3,131},{4,132},{5,133},{6,134},{7,135},{8... | collective-permute-start | bytes 776 | tf_op jit(solution)/shard_map/ppermute | solution.py:10
  163.9 7.3 %collective-permute-start.22 = (bf16[128,128]{1,0:T(8,128)(2,1)S(1)}, bf16[128,128]{1,0:T(8,128)(2,1)S(1)}, u32[]{:S(2)}, u32[]{:S(2)}) collective-permute-start(bf16[128,128]{1,0:T(8,128)(2,1)S(1)} %maximum_select_fusion.6), channel_id=1, source_target_pairs={{0,128},{1,129},{2,130},{3,131},{4,132},{5,133},{6,134},{7,135},{8... | collective-permute-start | bytes 98312 | tf_op jit(solution)/shard_map/ppermute | solution.py:10
  171.2 5.2 %collective-permute-start.28 = (bf16[256]{0:T(256)(128)(2,1)S(1)}, bf16[256]{0:T(256)(128)(2,1)S(1)}, u32[]{:S(2)}, u32[]{:S(2)}) collective-permute-start(bf16[256]{0:T(256)(128)(2,1)S(1)} %get-tuple-element.4), channel_id=1, source_target_pairs={{0,256},{1,257},{2,258},{3,259},{4,260},{5,261},{6,262},{7,263},{8... | collective-permute-start | bytes 1544 | tf_op jit(solution)/shard_map/ppermute | solution.py:10
  176.5 7.8 %collective-permute-done.28 = bf16[256]{0:T(256)(128)(2,1)S(1)} collective-permute-done((bf16[256]{0:T(256)(128)(2,1)S(1)}, bf16[256]{0:T(256)(128)(2,1)S(1)}, u32[]{:S(2)}, u32[]{:S(2)}) %collective-permute-start.28) | collective-permute-done | bytes 544 | tf_op jit(solution)/shard_map/ppermute | solution.py:10
  184.3 5.2 %collective-permute-start.23 = (bf16[256,128]{1,0:T(8,128)(2,1)S(1)}, bf16[256,128]{1,0:T(8,128)(2,1)S(1)}, u32[]{:S(2)}, u32[]{:S(2)}) collective-permute-start(bf16[256,128]{1,0:T(8,128)(2,1)S(1)} %maximum_select_fusion.4), channel_id=1, source_target_pairs={{0,256},{1,257},{2,258},{3,259},{4,260},{5,261},{6,262},{7,263},{8... | collective-permute-start | bytes 196616 | tf_op jit(solution)/shard_map/ppermute | solution.py:10
  189.5 8.5 %collective-permute-done.23 = bf16[256,128]{1,0:T(8,128)(2,1)S(1)} collective-permute-done((bf16[256,128]{1,0:T(8,128)(2,1)S(1)}, bf16[256,128]{1,0:T(8,128)(2,1)S(1)}, u32[]{:S(2)}, u32[]{:S(2)}) %collective-permute-start.23) | collective-permute-done | bytes 65568 | tf_op jit(solution)/shard_map/ppermute | solution.py:10
  203.3 3.0 %collective-permute-start.30 = (bf16[128,128]{1,0:T(8,128)(2,1)S(1)}, bf16[128,128]{1,0:T(8,128)(2,1)S(1)}, u32[]{:S(2)}, u32[]{:S(2)}) collective-permute-start(bf16[128,128]{1,0:T(8,128)(2,1)S(1)} %dynamic-slice_convert_fusion.4), channel_id=1, source_target_pairs={{0,4},{1,5},{2,6},{3,7},{4,0},{5,1},{6,2},{7,3},{8,12},{9,13},{10,... | collective-permute-start | bytes 98312 | tf_op jit(solution)/shard_map/ppermute | solution.py:10
  206.3 3.1 %collective-permute-done.30 = bf16[128,128]{1,0:T(8,128)(2,1)S(1)} collective-permute-done((bf16[128,128]{1,0:T(8,128)(2,1)S(1)}, bf16[128,128]{1,0:T(8,128)(2,1)S(1)}, u32[]{:S(2)}, u32[]{:S(2)}) %collective-permute-start.30) | collective-permute-done | bytes 32800 | tf_op jit(solution)/shard_map/ppermute | solution.py:10
  214.0 16.8 %collective-permute-start.32 = (bf16[32,128]{1,0:T(8,128)(2,1)S(1)}, bf16[32,128]{1,0:T(8,128)(2,1)S(1)}, u32[]{:S(2)}, u32[]{:S(2)}) collective-permute-start(bf16[32,128]{1,0:T(8,128)(2,1)S(1)} %dynamic-slice_convert_fusion.8), channel_id=1, source_target_pairs={{0,1},{1,0},{2,3},{3,2},{4,5},{5,4},{6,7},{7,6},{8,9},{9,8},{10,11... | collective-permute-start | bytes 24584 | tf_op jit(solution)/shard_map/ppermute | solution.py:10
  (138 shorter events, 66.0 us)
Async XLA Ops:
  0.6 9.8 %collective-permute-start = (bf16[32,128]{1,0:T(8,128)(2,1)}, bf16[32,128]{1,0:T(8,128)(2,1)S(1)}, u32[]{:S(2)}, u32[]{:S(2)}) collective-permute-start(bf16[32,128]{1,0:T(8,128)(2,1)} %param.12), channel_id=1, source_target_pairs={{0,1},{1,0},{2,3},{3,2},{4,5},{5,4},{6,7},{7,6},{8,9},{9,8},{10,11... | collective-permute-start | bytes 24584 | tf_op jit(solution)/shard_map/ppermute | solution.py:10
  26.4 14.3 %collective-permute-start.9 = (bf16[256]{0:T(256)(128)(2,1)S(1)}, bf16[256]{0:T(256)(128)(2,1)S(1)}, u32[]{:S(2)}, u32[]{:S(2)}) collective-permute-start(bf16[256]{0:T(256)(128)(2,1)S(1)} %dynamic_slice.235), channel_id=1, source_target_pairs={{0,256},{1,257},{2,258},{3,259},{4,260},{5,261},{6,262},{7,263},{8... | collective-permute-start | bytes 1544 | tf_op jit(solution)/shard_map/ppermute | solution.py:10
  38.4 28.5 %collective-permute-start.4 = (bf16[256,2]{0,1:T(2,128)(2,1)S(1)}, bf16[256,2]{0,1:T(2,128)(2,1)S(1)}, u32[]{:S(2)}, u32[]{:S(2)}) collective-permute-start(bf16[256,2]{0,1:T(2,128)(2,1)S(1)} %fusion.22), channel_id=1, source_target_pairs={{0,256},{1,257},{2,258},{3,259},{4,260},{5,261},{6,262},{7,263},{8... | collective-permute-start | bytes 3080 | tf_op jit(solution)/shard_map/ppermute | solution.py:10
  40.8 8.2 %collective-permute-start.10 = (bf16[128]{0:T(256)(128)(2,1)S(1)}, bf16[128]{0:T(256)(128)(2,1)S(1)}, u32[]{:S(2)}, u32[]{:S(2)}) collective-permute-start(bf16[128]{0:T(256)(128)(2,1)S(1)} %dynamic_slice.239), channel_id=1, source_target_pairs={{0,128},{1,129},{2,130},{3,131},{4,132},{5,133},{6,134},{7,135},{8... | collective-permute-start | bytes 776 | tf_op jit(solution)/shard_map/ppermute | solution.py:10
  49.2 14.9 %collective-permute-start.11 = (bf16[64]{0:T(256)(128)(2,1)S(1)}, bf16[64]{0:T(256)(128)(2,1)S(1)}, u32[]{:S(2)}, u32[]{:S(2)}) collective-permute-start(bf16[64]{0:T(256)(128)(2,1)S(1)} %dynamic_slice.238), channel_id=1, source_target_pairs={{0,64},{1,65},{2,66},{3,67},{4,68},{5,69},{6,70},{7,71},{8,72},{9,... | collective-permute-start | bytes 392 | tf_op jit(solution)/shard_map/ppermute | solution.py:10
  52.0 44.5 %collective-permute-start.14 = (bf16[256,512]{1,0:T(8,128)(2,1)S(1)}, bf16[256,512]{1,0:T(8,128)(2,1)S(1)}, u32[]{:S(2)}, u32[]{:S(2)}) collective-permute-start(bf16[256,512]{1,0:T(8,128)(2,1)S(1)} %dynamic-slice_convert_fusion), channel_id=1, source_target_pairs={{0,256},{1,257},{2,258},{3,259},{4,260},{5,261},{6,262},{7,263},{8... | collective-permute-start | bytes 786440 | tf_op jit(solution)/shard_map/ppermute | solution.py:10
  64.2 12.3 %collective-permute-start.12 = (bf16[32]{0:T(256)(128)(2,1)S(1)}, bf16[32]{0:T(256)(128)(2,1)S(1)}, u32[]{:S(2)}, u32[]{:S(2)}) collective-permute-start(bf16[32]{0:T(256)(128)(2,1)S(1)} %dynamic_slice.237), channel_id=1, source_target_pairs={{0,32},{1,33},{2,34},{3,35},{4,36},{5,37},{6,38},{7,39},{8,40},{9,... | collective-permute-start | bytes 200 | tf_op jit(solution)/shard_map/ppermute | solution.py:10
  66.9 14.5 %collective-permute-start.5 = (bf16[128,2]{0,1:T(2,128)(2,1)S(1)}, bf16[128,2]{0,1:T(2,128)(2,1)S(1)}, u32[]{:S(2)}, u32[]{:S(2)}) collective-permute-start(bf16[128,2]{0,1:T(2,128)(2,1)S(1)} %fusion.24), channel_id=1, source_target_pairs={{0,128},{1,129},{2,130},{3,131},{4,132},{5,133},{6,134},{7,135},{8... | collective-permute-start | bytes 1544 | tf_op jit(solution)/shard_map/ppermute | solution.py:10
  76.6 8.0 %collective-permute-start.13 = (bf16[16]{0:T(256)(128)(2,1)S(1)}, bf16[16]{0:T(256)(128)(2,1)S(1)}, u32[]{:S(2)}, u32[]{:S(2)}) collective-permute-start(bf16[16]{0:T(256)(128)(2,1)S(1)} %dynamic_slice.236), channel_id=1, source_target_pairs={{0,16},{1,17},{2,18},{3,19},{4,20},{5,21},{6,22},{7,23},{8,24},{9,... | collective-permute-start | bytes 104 | tf_op jit(solution)/shard_map/ppermute | solution.py:10
  87.0 16.8 %collective-permute-start.7 = (bf16[32,2]{0,1:T(2,128)(2,1)S(1)}, bf16[32,2]{0,1:T(2,128)(2,1)S(1)}, u32[]{:S(2)}, u32[]{:S(2)}) collective-permute-start(bf16[32,2]{0,1:T(2,128)(2,1)S(1)} %fusion.28), channel_id=1, source_target_pairs={{0,32},{1,33},{2,34},{3,35},{4,36},{5,37},{6,38},{7,39},{8,40},{9,... | collective-permute-start | bytes 392 | tf_op jit(solution)/shard_map/ppermute | solution.py:10
  96.6 13.7 %collective-permute-start.15 = (bf16[128,512]{1,0:T(8,128)(2,1)S(1)}, bf16[128,512]{1,0:T(8,128)(2,1)S(1)}, u32[]{:S(2)}, u32[]{:S(2)}) collective-permute-start(bf16[128,512]{1,0:T(8,128)(2,1)S(1)} %dynamic-slice_convert_fusion.1), channel_id=1, source_target_pairs={{0,128},{1,129},{2,130},{3,131},{4,132},{5,133},{6,134},{7,135},{8... | collective-permute-start | bytes 393224 | tf_op jit(solution)/shard_map/ppermute | solution.py:10
  104.0 8.3 %collective-permute-start.8 = (bf16[16,2]{0,1:T(2,128)(2,1)S(1)}, bf16[16,2]{0,1:T(2,128)(2,1)S(1)}, u32[]{:S(2)}, u32[]{:S(2)}) collective-permute-start(bf16[16,2]{0,1:T(2,128)(2,1)S(1)} %fusion.32), channel_id=1, source_target_pairs={{0,16},{1,17},{2,18},{3,19},{4,20},{5,21},{6,22},{7,23},{8,24},{9,... | collective-permute-start | bytes 200 | tf_op jit(solution)/shard_map/ppermute | solution.py:10
  110.4 6.8 %collective-permute-start.16 = (bf16[64,512]{1,0:T(8,128)(2,1)S(1)}, bf16[64,512]{1,0:T(8,128)(2,1)S(1)}, u32[]{:S(2)}, u32[]{:S(2)}) collective-permute-start(bf16[64,512]{1,0:T(8,128)(2,1)S(1)} %dynamic-slice_convert_fusion.3), channel_id=1, source_target_pairs={{0,64},{1,65},{2,66},{3,67},{4,68},{5,69},{6,70},{7,71},{8,72},{9,... | collective-permute-start | bytes 196616 | tf_op jit(solution)/shard_map/ppermute | solution.py:10
  122.9 9.6 %collective-permute-start.18 = (bf16[16,512]{1,0:T(8,128)(2,1)S(1)}, bf16[16,512]{1,0:T(8,128)(2,1)S(1)}, u32[]{:S(2)}, u32[]{:S(2)}) collective-permute-start(bf16[16,512]{1,0:T(8,128)(2,1)S(1)} %dynamic-slice_convert_fusion.7), channel_id=1, source_target_pairs={{0,16},{1,17},{2,18},{3,19},{4,20},{5,21},{6,22},{7,23},{8,24},{9,... | collective-permute-start | bytes 49160 | tf_op jit(solution)/shard_map/ppermute | solution.py:10
  133.9 6.8 %collective-permute-start.24 = (bf16[16]{0:T(256)(128)(2,1)S(1)}, bf16[16]{0:T(256)(128)(2,1)S(1)}, u32[]{:S(2)}, u32[]{:S(2)}) collective-permute-start(bf16[16]{0:T(256)(128)(2,1)S(1)} %get-tuple-element.19), channel_id=1, source_target_pairs={{0,16},{1,17},{2,18},{3,19},{4,20},{5,21},{6,22},{7,23},{8,24},{9,... | collective-permute-start | bytes 104 | tf_op jit(solution)/shard_map/ppermute | solution.py:10
  138.8 6.3 %collective-permute-start.19 = (bf16[16,128]{1,0:T(8,128)(2,1)S(1)}, bf16[16,128]{1,0:T(8,128)(2,1)S(1)}, u32[]{:S(2)}, u32[]{:S(2)}) collective-permute-start(bf16[16,128]{1,0:T(8,128)(2,1)S(1)} %get-tuple-element.15), channel_id=1, source_target_pairs={{0,16},{1,17},{2,18},{3,19},{4,20},{5,21},{6,22},{7,23},{8,24},{9,... | collective-permute-start | bytes 12296 | tf_op jit(solution)/shard_map/ppermute | solution.py:10
  145.1 7.2 %collective-permute-start.20 = (bf16[32,128]{1,0:T(8,128)(2,1)S(1)}, bf16[32,128]{1,0:T(8,128)(2,1)S(1)}, u32[]{:S(2)}, u32[]{:S(2)}) collective-permute-start(bf16[32,128]{1,0:T(8,128)(2,1)S(1)} %maximum_select_fusion.9), channel_id=1, source_target_pairs={{0,32},{1,33},{2,34},{3,35},{4,36},{5,37},{6,38},{7,39},{8,40},{9,... | collective-permute-start | bytes 24584 | tf_op jit(solution)/shard_map/ppermute | solution.py:10
  152.3 11.6 %collective-permute-start.21 = (bf16[64,128]{1,0:T(8,128)(2,1)S(1)}, bf16[64,128]{1,0:T(8,128)(2,1)S(1)}, u32[]{:S(2)}, u32[]{:S(2)}) collective-permute-start(bf16[64,128]{1,0:T(8,128)(2,1)S(1)} %maximum_select_fusion.8), channel_id=1, source_target_pairs={{0,64},{1,65},{2,66},{3,67},{4,68},{5,69},{6,70},{7,71},{8,72},{9,... | collective-permute-start | bytes 49160 | tf_op jit(solution)/shard_map/ppermute | solution.py:10
  154.7 9.2 %collective-permute-start.27 = (bf16[128]{0:T(256)(128)(2,1)S(1)}, bf16[128]{0:T(256)(128)(2,1)S(1)}, u32[]{:S(2)}, u32[]{:S(2)}) collective-permute-start(bf16[128]{0:T(256)(128)(2,1)S(1)} %get-tuple-element.6), channel_id=1, source_target_pairs={{0,128},{1,129},{2,130},{3,131},{4,132},{5,133},{6,134},{7,135},{8... | collective-permute-start | bytes 776 | tf_op jit(solution)/shard_map/ppermute | solution.py:10
  163.9 20.3 %collective-permute-start.22 = (bf16[128,128]{1,0:T(8,128)(2,1)S(1)}, bf16[128,128]{1,0:T(8,128)(2,1)S(1)}, u32[]{:S(2)}, u32[]{:S(2)}) collective-permute-start(bf16[128,128]{1,0:T(8,128)(2,1)S(1)} %maximum_select_fusion.6), channel_id=1, source_target_pairs={{0,128},{1,129},{2,130},{3,131},{4,132},{5,133},{6,134},{7,135},{8... | collective-permute-start | bytes 98312 | tf_op jit(solution)/shard_map/ppermute | solution.py:10
  171.2 13.0 %collective-permute-start.28 = (bf16[256]{0:T(256)(128)(2,1)S(1)}, bf16[256]{0:T(256)(128)(2,1)S(1)}, u32[]{:S(2)}, u32[]{:S(2)}) collective-permute-start(bf16[256]{0:T(256)(128)(2,1)S(1)} %get-tuple-element.4), channel_id=1, source_target_pairs={{0,256},{1,257},{2,258},{3,259},{4,260},{5,261},{6,262},{7,263},{8... | collective-permute-start | bytes 1544 | tf_op jit(solution)/shard_map/ppermute | solution.py:10
  184.3 13.7 %collective-permute-start.23 = (bf16[256,128]{1,0:T(8,128)(2,1)S(1)}, bf16[256,128]{1,0:T(8,128)(2,1)S(1)}, u32[]{:S(2)}, u32[]{:S(2)}) collective-permute-start(bf16[256,128]{1,0:T(8,128)(2,1)S(1)} %maximum_select_fusion.4), channel_id=1, source_target_pairs={{0,256},{1,257},{2,258},{3,259},{4,260},{5,261},{6,262},{7,263},{8... | collective-permute-start | bytes 196616 | tf_op jit(solution)/shard_map/ppermute | solution.py:10
  203.3 6.2 %collective-permute-start.30 = (bf16[128,128]{1,0:T(8,128)(2,1)S(1)}, bf16[128,128]{1,0:T(8,128)(2,1)S(1)}, u32[]{:S(2)}, u32[]{:S(2)}) collective-permute-start(bf16[128,128]{1,0:T(8,128)(2,1)S(1)} %dynamic-slice_convert_fusion.4), channel_id=1, source_target_pairs={{0,4},{1,5},{2,6},{3,7},{4,0},{5,1},{6,2},{7,3},{8,12},{9,13},{10,... | collective-permute-start | bytes 98312 | tf_op jit(solution)/shard_map/ppermute | solution.py:10
  214.0 17.6 %collective-permute-start.32 = (bf16[32,128]{1,0:T(8,128)(2,1)S(1)}, bf16[32,128]{1,0:T(8,128)(2,1)S(1)}, u32[]{:S(2)}, u32[]{:S(2)}) collective-permute-start(bf16[32,128]{1,0:T(8,128)(2,1)S(1)} %dynamic-slice_convert_fusion.8), channel_id=1, source_target_pairs={{0,1},{1,0},{2,3},{3,2},{4,5},{5,4},{6,7},{7,6},{8,9},{9,8},{10,11... | collective-permute-start | bytes 24584 | tf_op jit(solution)/shard_map/ppermute | solution.py:10
  (19 other events, 424.5 us)
where the time goes:
time: 233 us; the launch traced here: 232 us
  starting transfers between devices  162 us (70%)
  waiting for transfers between devices  60.1 us (26%)
  other arithmetic  3.56 us (2%)
  local copies, waits for them, and re-layouts  2.97 us (1%)
  between operations  2.38 us (1%)
    ppermute x33, starting transfers between devices, from_partner(): lax.ppermute(shard, axis, [(i, i ^ 1 << bit) for i in range(lax.axis_size...  162 us
    ppermute x33, waiting for transfers between devices, from_partner(): lax.ppermute(shard, axis, [(i, i ^ 1 << bit) for i in range(lax.axis_size...  60.1 us
  transfers between devices with their start and end apart: 33, of which 20 were waited for; matrix products, arithmetic and copies ran while one was open for 2% of the time, Pallas kernels for 0%

commit v1 on v0

v1 whole, which is shorter than its diff:
```python
import jax
import jax.numpy as jnp
from jax import lax
from jax.sharding import Mesh, PartitionSpec as P

EPS = 1e-06
PAIR = 2


def per_device(
    stream,
    norm_gain,
    query_weight,
    key_weight,
    value_weight,
    gate_weight,
    write_weight,
    decay_weight,
    decay_rate,
    head_gain,
    out_weight,
    state,
):
    f32, bf16 = jnp.float32, jnp.bfloat16
    planes = lax.axis_size("z")
    heads = lax.axis_size("h")
    my_z, my_y, my_h = lax.axis_index("z"), lax.axis_index("y"), lax.axis_index("h")
    rows, cols = stream.shape
    half = rows // PAIR
    width = cols * PAIR * planes
    size = head_gain.shape[0]
    seqs = half * planes

    own = jnp.stack([query_weight, key_weight, value_weight, gate_weight, out_weight])
    other = lax.ppermute(own, "y", [(0, 1), (1, 0)])

    blocks = jnp.broadcast_to(stream.reshape(PAIR, 1, half, cols), (PAIR, heads, half, cols))
    got = lax.all_to_all(blocks.reshape(PAIR * heads, half, cols), ("y", "h"), 0, 0)
    got = got.reshape(PAIR, seqs, cols)
    first = lax.dynamic_slice_in_dim(got, my_y, 1, 0)[0]
    second = lax.dynamic_slice_in_dim(got, 1 - my_y, 1, 0)[0]
    small_w = jnp.concatenate([write_weight, decay_weight], axis=1)

    def gained_of(block, place):
        start = (my_z * PAIR + place) * cols
        gain = lax.dynamic_slice_in_dim(norm_gain, start, cols, 0).astype(f32)
        return (block.astype(f32) * gain[None, :]).astype(bf16)

    def small_of(place):
        start = (my_z * PAIR + place) * cols
        return lax.dynamic_slice_in_dim(small_w, start, cols, 0)

    first_g, second_g = gained_of(first, my_y), gained_of(second, 1 - my_y)

    def dot(a, b):
        return jnp.dot(a, b, preferred_element_type=f32)

    small = dot(first_g, small_of(my_y)) + dot(second_g, small_of(1 - my_y))
    picked = jnp.arange(2 * heads)[None, :] % heads == my_h
    small = jnp.where(picked, small, 0.0).reshape(seqs, 2, heads).sum(axis=2)
    squares = jnp.sum(got.astype(f32) ** 2, axis=(0, 2))
    small = jnp.concatenate([small, squares[:, None]], axis=1)
    small = jnp.pad(small.reshape(planes, PAIR, half // PAIR, 3), ((0, 0), (0, 0), (0, 0), (0, 61)))
    small = small.transpose(0, 2, 1, 3).reshape(planes, half // PAIR, 128).astype(bf16)
    parts = [
        (dot(first_g, own[m]) + dot(second_g, other[m])).astype(bf16).reshape(planes, half, size)
        for m in range(4)
    ]
    packed = jnp.concatenate(parts + [small], axis=1)
    summed = lax.all_to_all(packed, "z", 0, 0).astype(f32).sum(axis=0)

    tail = summed[4 * half :].reshape(half // PAIR, PAIR, 64).transpose(1, 0, 2).reshape(half, 64)
    row_scale = lax.rsqrt(tail[:, 2] / width + EPS)

    def scaled(value):
        return (value * row_scale[:, None]).astype(bf16).astype(f32)

    query_raw, key_raw, value_vec, gate_vec = [
        scaled(summed[m * half : (m + 1) * half]) for m in range(4)
    ]
    small_pre = scaled(tail[:, :2])
    query_vec = (
        query_raw
        * lax.rsqrt(jnp.sum(query_raw * query_raw, axis=-1, keepdims=True) + EPS)
        * size ** (-0.5)
    )
    key_vec = key_raw * lax.rsqrt(jnp.sum(key_raw * key_raw, axis=-1, keepdims=True) + EPS)
    strength = jax.nn.sigmoid(small_pre[:, 0])
    rate = lax.dynamic_slice_in_dim(decay_rate, my_h, 1, 0)[0]
    factor = jnp.exp(-rate * jax.nn.softplus(small_pre[:, 1]))
    recalled = jnp.sum(state * key_vec[:, :, None], axis=1)
    correction = strength[:, None] * (value_vec - factor[:, None] * recalled)
    updated = factor[:, None, None] * state + key_vec[:, :, None] * correction[:, None, :]
    readout = jnp.sum(updated * query_vec[:, :, None], axis=1)
    scaling = lax.rsqrt(jnp.mean(readout * readout, axis=1, keepdims=True) + EPS)
    gated = (scaling * readout * head_gain.astype(f32)[None, :] * jax.nn.silu(gate_vec)).astype(bf16)

    spread = jnp.broadcast_to(gated[None], (planes, half, size))
    all_gated = lax.all_to_all(spread, "z", 0, 0).reshape(seqs, size)

    def project(weight):
        return lax.dot_general(
            all_gated, weight, (((1,), (1,)), ((), ())), preferred_element_type=f32
        ).astype(bf16)

    own_out, other_out = project(own[4]), project(other[4])
    low = jnp.where(my_y == 0, own_out, other_out)
    high = jnp.where(my_y == 0, other_out, own_out)
    outs = jnp.stack([low, high]).reshape(PAIR * heads, half, cols)
    terms = lax.all_to_all(outs, ("y", "h"), 0, 0).reshape(PAIR, heads, half, cols)
    result = terms.astype(f32).sum(axis=1).reshape(rows, cols) + stream.astype(f32)
    return result.astype(bf16), updated


def solution(mesh):
    heads = 16
    grid = Mesh(mesh.devices.reshape(-1, PAIR, heads), ("z", "y", "h"))
    every = ("z", "y", "h")
    flat, cube, same = P(every, None), P(every, None, None), P()
    placed = (flat, same, flat, flat, flat, flat, same, same, same, same, flat, cube)
    return jax.shard_map(
        per_device, mesh=grid, in_specs=placed, out_specs=(flat, cube), check_vma=False
    )
```

time: 233 us -> 101 us (0.43)
  starting transfers between devices: 162 us -> 40.3 us
  waiting for transfers between devices: 60.1 us -> 23.2 us
  blocking collectives: 0 us -> 16.4 us
  local copies, waits for them, and re-layouts: 2.97 us -> 12.1 us
    ppermute x33 -> x1, starting transfers between devices: 162 us -> 4.86 us  [per_device(): other = lax.ppermute(own, 'y', [(0, 1), (1, 0)])]
    ppermute x33 -> x1, waiting for transfers between devices: 60.1 us -> 0.01 us  [per_device(): other = lax.ppermute(own, 'y', [(0, 1), (1, 0)])]
    all_to_all x0 -> x3, starting transfers between devices: none -> 35.4 us  [the longest x1 13 us: per_device(): summed = lax.all_to_all(packed, 'z', 0, 0).astype(f32).sum(axis=0)]
    all_to_all x0 -> x3, waiting for transfers between devices: none -> 23.2 us  [the longest x1 11.6 us: per_device(): summed = lax.all_to_all(packed, 'z', 0, 0).astype(f32).sum(axis=0)]
    all_to_all x0 -> x1, blocking collectives: none -> 16.4 us  [per_device(): lax.all_to_all(outs, ('y', 'h'), 0, 0).reshape(PAIR, heads, half, cols)]
    unnamed x20 -> x31, local copies, waits for them, and re-layouts: 0.05 us -> 7.84 us
  transfers between devices with their start and end apart: 33 -> 4, of which waited for: 20 -> 2; matrix products, arithmetic and copies ran while one was open for 2% -> 4% of each run, Pallas kernels for 0% -> 0%
where the time goes in v1:
time: 101 us; the launch traced here: 100 us
  starting transfers between devices  40.3 us (40%)
  waiting for transfers between devices  23.2 us (23%)
  blocking collectives  16.4 us (16%)
  local copies, waits for them, and re-layouts  12.1 us (12%)
  other arithmetic  4.92 us (5%)
  matrix products  1.81 us (2%)
  between operations  1.62 us (2%)
    all_to_all x1, blocking collectives, per_device(): lax.all_to_all(outs, ('y', 'h'), 0, 0).reshape(PAIR, heads, half, cols)  16.4 us
    all_to_all x1, starting transfers between devices, per_device(): summed = lax.all_to_all(packed, 'z', 0, 0).astype(f32).sum(axis=0)  13 us
    all_to_all x1, starting transfers between devices, per_device(): all_gated = lax.all_to_all(spread, 'z', 0, 0).reshape(seqs, size)  11.9 us
    all_to_all x1, waiting for transfers between devices, per_device(): summed = lax.all_to_all(packed, 'z', 0, 0).astype(f32).sum(axis=0)  11.6 us
    all_to_all x1, waiting for transfers between devices, per_device(): all_gated = lax.all_to_all(spread, 'z', 0, 0).reshape(seqs, size)  11.6 us
    all_to_all x1, starting transfers between devices, per_device(): lax.all_to_all(blocks.reshape(PAIR * heads, half, cols), ('y', 'h'), 0, 0)  10.5 us
    unnamed x31, local copies, waits for them, and re-layouts  7.84 us
    ppermute x1, starting transfers between devices, per_device(): other = lax.ppermute(own, 'y', [(0, 1), (1, 0)])  4.86 us
  transfers between devices with their start and end apart: 4, of which 2 were waited for; matrix products, arithmetic and copies ran while one was open for 4% of the time, Pallas kernels for 0%

profile of v1, /device:TPU:1, one launch (start us, length us, event | category | flops | bytes accessed | tf_op | source)
XLA Modules:
  0.0 100.3 jit_solution(5687299235974024383)
XLA Ops:
  0.6 1.4 %broadcast_in_dim.19 = bf16[2,16,16,128]{3,2,1,0:T(8,128)(2,1)} broadcast(bf16[2,16,128]{2,1,0:T(8,128)(2,1)} %bitcast.107), dimensions={0,2,3} | broadcast | bytes 139264 | tf_op jit(solution)/shard_map/broadcast_in_dim | solution.py:37
  2.0 10.5 %all-to-all-start = ((bf16[32,16,128]{2,1,0:T(8,128)(2,1)}), bf16[32,16,128]{2,1,0:T(8,128)(2,1)S(1)}, u32[]{:S(2)}, u32[]{:S(2)}) async-start(bf16[32,16,128]{2,1,0:T(8,128)(2,1)} %bitcast.2), calls=%async_computation | async-start | bytes 262144 | tf_op jit(solution)/shard_map/all_to_all | solution.py:38
  12.5 0.7 copy-done.1
  13.3 0.7 copy-done.2
  14.0 0.7 copy-done.3
  14.8 0.7 copy-done.5
  15.6 4.9 %collective-permute-start = (bf16[5,128,128]{2,1,0:T(8,128)(2,1)S(1)}, bf16[5,128,128]{2,1,0:T(8,128)(2,1)S(1)}, u32[]{:S(2)}, u32[]{:S(2)}) collective-permute-start(bf16[5,128,128]{2,1,0:T(8,128)(2,1)S(1)} %bitcast_dynamic-update-slice_fusion), channel_id=1, source_target_pairs={{0,16},{16,0},{1,17},{17,1},{2,18},{18,2},{3,19},{19,3},{4,20},{20... | collective-permute-start | bytes 491528 | tf_op jit(solution)/shard_map/ppermute | solution.py:35
  20.5 0.9 copy-done.7
  21.4 0.8 dynamic-slice_convert_fusion
  24.7 0.6 constant_dynamic-update-slice_fusion.6
  25.5 0.6 constant_dynamic-update-slice_fusion.5
  26.3 0.6 constant_dynamic-update-slice_fusion.4
  27.1 0.6 constant_dynamic-update-slice_fusion.3
  27.8 0.6 constant_dynamic-update-slice_fusion.2
  28.4 13.0 %all-to-all-start.1 = ((bf16[16,72,128]{2,1,0:T(8,128)(2,1)}), bf16[16,72,128]{2,1,0:T(8,128)(2,1)S(1)}, u32[]{:S(2)}, u32[]{:S(2)}) async-start(bf16[16,72,128]{2,1,0:T(8,128)(2,1)} %constant_dynamic-update-slice_fusion.2), calls=%async_computation.1 | async-start | bytes 589824 | tf_op jit(solution)/shard_map/all_to_all | solution.py:70
  41.5 0.6 copy-done.9
  43.4 11.6 %all-to-all-done.1 = bf16[16,72,128]{2,1,0:T(8,128)(2,1)S(1)} async-done(((bf16[16,72,128]{2,1,0:T(8,128)(2,1)}), bf16[16,72,128]{2,1,0:T(8,128)(2,1)S(1)}, u32[]{:S(2)}, u32[]{:S(2)}) %all-to-all-start.1) | async-done | bytes 294944 | tf_op jit(solution)/shard_map/all_to_all | solution.py:70
  56.4 1.5 %multiply_reduce_fusion = (f32[16,128]{1,0:T(8,128)S(1)}, f32[16,128,128]{2,1,0:T(8,128)}) fusion(f32[16,128]{1,0:T(8,128)S(1)} %get-tuple-element.12, f32[16,128]{1,0:T(8,128)S(1)} %get-tuple-element.11, f32[16,128]{1,0:T(8,128)S(1)} %convert_multiply_fusion.5, f32[16,128,128]{2,1,0:T(8,128)S(1)} %copy-done, f32[16]{0:T(128)S(1)} %fusion.72), kind=kLoop, calls=%fused_computation.15 | loop fusion | flops 1308672 | bytes 2129984 | tf_op jit(solution)/shard_map/reduce_sum | solution.py:94
  58.1 0.6 broadcast_in_dim.22
  58.7 11.9 %all-to-all-start.2 = ((bf16[16,16,128]{2,1,0:T(8,128)(2,1)}), bf16[16,16,128]{2,1,0:T(8,128)(2,1)S(1)}, u32[]{:S(2)}, u32[]{:S(2)}) async-start(bf16[16,16,128]{2,1,0:T(8,128)(2,1)} %broadcast_in_dim.22), calls=%async_computation.2 | async-start | bytes 131072 | tf_op jit(solution)/shard_map/all_to_all | solution.py:99
  70.7 11.6 %all-to-all-done.2 = bf16[16,16,128]{2,1,0:T(8,128)(2,1)S(1)} async-done(((bf16[16,16,128]{2,1,0:T(8,128)(2,1)}), bf16[16,16,128]{2,1,0:T(8,128)(2,1)S(1)}, u32[]{:S(2)}, u32[]{:S(2)}) %all-to-all-start.2) | async-done | bytes 65568 | tf_op jit(solution)/shard_map/all_to_all | solution.py:99
  82.6 16.4 %all_to_all.20 = bf16[32,16,128]{2,1,0:T(8,128)(2,1)S(1)} all-to-all(bf16[32,16,128]{2,1,0:T(8,128)(2,1)S(1)} %bitcast.100), channel_id=1, replica_groups=mesh['z'=16,'y'=2,'h'=16] {'y','h'}, dimensions={0} | all-to-all | bytes 262144 | tf_op jit(solution)/shard_map/all_to_all | solution.py:110
  99.1 0.7 copy-done.8
  99.7 0.6 fusion.21
  (65 shorter events, 5.4 us)
Async XLA Ops:
  2.0 10.5 %copy-start.4 = (bf16[128,128]{1,0:T(8,128)(2,1)S(1)}, bf16[128,128]{1,0:T(8,128)(2,1)}, u32[]{:S(2)}) copy-start(bf16[128,128]{1,0:T(8,128)(2,1)} %param.14) | copy-start | bytes 98308
  2.0 18.4 %copy-start.6 = (bf16[4096,16]{0,1:T(8,128)(2,1)S(1)}, bf16[4096,16]{0,1:T(8,128)(2,1)}, u32[]{:S(2)}) copy-start(bf16[4096,16]{0,1:T(8,128)(2,1)} %param.18) | copy-start | bytes 393220
  2.0 20.2 %all-to-all-start = ((bf16[32,16,128]{2,1,0:T(8,128)(2,1)}), bf16[32,16,128]{2,1,0:T(8,128)(2,1)S(1)}, u32[]{:S(2)}, u32[]{:S(2)}) async-start(bf16[32,16,128]{2,1,0:T(8,128)(2,1)} %bitcast.2), calls=%async_computation | async-start | bytes 262144 | tf_op jit(solution)/shard_map/all_to_all | solution.py:38
  12.5 0.8 copy-start.1
  13.3 0.8 copy-start.2
  14.0 0.8 copy-start.3
  14.8 0.8 copy-start.5
  15.6 9.0 %collective-permute-start = (bf16[5,128,128]{2,1,0:T(8,128)(2,1)S(1)}, bf16[5,128,128]{2,1,0:T(8,128)(2,1)S(1)}, u32[]{:S(2)}, u32[]{:S(2)}) collective-permute-start(bf16[5,128,128]{2,1,0:T(8,128)(2,1)S(1)} %bitcast_dynamic-update-slice_fusion), channel_id=1, source_target_pairs={{0,16},{16,0},{1,17},{17,1},{2,18},{18,2},{3,19},{19,3},{4,20},{20... | collective-permute-start | bytes 491528 | tf_op jit(solution)/shard_map/ppermute | solution.py:35
  20.4 0.9 copy-start.7
  25.5 30.4 %copy-start = (f32[16,128,128]{2,1,0:T(8,128)S(1)}, f32[16,128,128]{2,1,0:T(8,128)}, u32[]{:S(2)}) copy-start(f32[16,128,128]{2,1,0:T(8,128)} %param.23) | copy-start | bytes 3145732
  28.4 26.6 %all-to-all-start.1 = ((bf16[16,72,128]{2,1,0:T(8,128)(2,1)}), bf16[16,72,128]{2,1,0:T(8,128)(2,1)S(1)}, u32[]{:S(2)}, u32[]{:S(2)}) async-start(bf16[16,72,128]{2,1,0:T(8,128)(2,1)} %constant_dynamic-update-slice_fusion.2), calls=%async_computation.1 | async-start | bytes 589824 | tf_op jit(solution)/shard_map/all_to_all | solution.py:70
  41.4 0.7 copy-start.9
  42.7 0.7 copy-start.10
  58.7 23.5 %all-to-all-start.2 = ((bf16[16,16,128]{2,1,0:T(8,128)(2,1)}), bf16[16,16,128]{2,1,0:T(8,128)(2,1)S(1)}, u32[]{:S(2)}, u32[]{:S(2)}) async-start(bf16[16,16,128]{2,1,0:T(8,128)(2,1)} %broadcast_in_dim.22), calls=%async_computation.2 | async-start | bytes 131072 | tf_op jit(solution)/shard_map/all_to_all | solution.py:99
  99.0 0.7 copy-start.8

commit v2 on v1

v2 whole, which is shorter than its diff:
```python
import jax
import jax.numpy as jnp
from jax import lax
from jax.experimental import pallas as pl
from jax.experimental.pallas import tpu as pltpu
from jax.sharding import Mesh, PartitionSpec as P

EPS = 1e-06
PAIR = 2
PARTS = 4
f32, bf16 = jnp.float32, jnp.bfloat16


def row_of(values, index):
    here = lax.broadcasted_iota(jnp.int32, values.shape, 0) == index
    return jnp.sum(jnp.where(here, values, 0.0), axis=0, keepdims=True)


def dot_t(a, b):
    return lax.dot_general(a, b, (((1,), (1,)), ((), ())), preferred_element_type=f32)


def stage_kernel(
    x_hbm, gain_hbm, write_hbm, decay_hbm, rate_hbm, head_gain_hbm, *refs
):
    weights, (blocks_ref, own_ref, x_ref, misc_ref), scratch = refs[:5], refs[5:9], refs[9:]
    gain_ref, write_ref, decay_ref, rate_ref, head_gain_ref, sems = scratch
    half = blocks_ref.shape[1]
    heads = blocks_ref.shape[0] // PAIR
    cols = blocks_ref.shape[2]
    my_z, my_y, my_h = lax.axis_index("z"), lax.axis_index("y"), lax.axis_index("h")
    here = pl.ds(pl.multiple_of(my_z * (PAIR * cols), PAIR * cols), PAIR * cols)
    moves = [(x_hbm, x_ref)] + [(ref, own_ref.at[m]) for m, ref in enumerate(weights)]
    moves += [
        (gain_hbm, gain_ref),
        (write_hbm.at[:, here], write_ref),
        (decay_hbm.at[:, here], decay_ref),
        (rate_hbm, rate_ref),
        (head_gain_hbm, head_gain_ref),
    ]
    copies = [pltpu.make_async_copy(a, b, sems.at[i]) for i, (a, b) in enumerate(moves)]
    for copy in copies:
        copy.start()
    copies[0].wait()
    for place in range(PAIR):
        rows = x_ref[place * half : (place + 1) * half, :]
        for head in range(heads):
            blocks_ref[place * heads + head] = rows
    for copy in copies[1:]:
        copy.wait()
    gains = gain_ref[...].astype(f32)
    lines = [row_of(gains, my_z * PAIR + place) for place in (my_y, 1 - my_y)]
    lines.append(head_gain_ref[...].astype(f32))
    rates = rate_ref[...]
    lane = lax.broadcasted_iota(jnp.int32, rates.shape, 1)
    rate = jnp.sum(jnp.where(lane == my_h, rates, 0.0), axis=1, keepdims=True)
    lines.append(jnp.broadcast_to(rate, (1, cols)))
    for ref in (write_ref, decay_ref):
        row = row_of(ref[...].astype(f32), my_h)
        low, high = row[:, :cols], row[:, cols:]
        lines.append(jnp.where(my_y == 0, low, high))
        lines.append(jnp.where(my_y == 0, high, low))
    for i, line in enumerate(lines):
        misc_ref[i : i + 1, :] = line


def project_kernel(got_ref, own_ref, other_ref, misc_ref, packed_ref):
    planes, half = packed_ref.shape[0], got_ref.shape[1]
    cols = got_ref.shape[2]
    heads = got_ref.shape[0] // PAIR
    seqs = heads * half
    my_y = lax.axis_index("y")
    squares, gained, small = None, [], None
    for i, place in enumerate((my_y, 1 - my_y)):
        x = got_ref[pl.ds(place * heads, heads)].reshape(seqs, cols).astype(f32)
        g = (x * misc_ref[i : i + 1, :]).astype(bf16)
        gained.append(g)
        squares = x * x if squares is None else squares + x * x
        line = lax.broadcasted_iota(jnp.int32, (128, cols), 0)
        write_row, decay_row = misc_ref[4 + i : 5 + i, :], misc_ref[6 + i : 7 + i, :]
        rows = jnp.where(line == 0, write_row, jnp.where(line == 1, decay_row, 0.0)).astype(bf16)
        term = dot_t(g, rows)
        small = term if small is None else small + term
    for m in range(PARTS):
        part = jnp.dot(gained[0], own_ref[m], preferred_element_type=f32)
        part = part + jnp.dot(gained[1], other_ref[m], preferred_element_type=f32)
        packed_ref[:, m * half : (m + 1) * half, :] = part.astype(bf16).reshape(planes, half, -1)
    total = jnp.sum(squares, axis=1, keepdims=True)
    lane = lax.broadcasted_iota(jnp.int32, small.shape, 1)
    small = jnp.where(lane == 2, total, small).reshape(planes, PAIR, half // PAIR, 128)
    tail = small[:, 0] + pltpu.roll(small[:, 1].reshape(-1, 128), 64, 1).reshape(planes, -1, 128)
    packed_ref[:, PARTS * half :, :] = tail.astype(bf16)


def state_kernel(width, recv_ref, state_ref, misc_ref, spread_ref, updated_ref):
    planes, half, size = spread_ref.shape
    summed = recv_ref[0].astype(f32)
    for z in range(1, planes):
        summed = summed + recv_ref[z].astype(f32)
    tail = summed[PARTS * half :]
    tail = jnp.concatenate([tail, pltpu.roll(tail, 64, 1)], axis=0)
    row_scale = lax.rsqrt(tail[:, 2:3] / width + EPS)

    def scaled(value):
        return (value * row_scale).astype(bf16).astype(f32)

    query, key, value, gate = [scaled(summed[m * half : (m + 1) * half]) for m in range(PARTS)]
    pre = scaled(tail)
    query = query * lax.rsqrt(jnp.sum(query * query, axis=1, keepdims=True) + EPS) * size**-0.5
    key = key * lax.rsqrt(jnp.sum(key * key, axis=1, keepdims=True) + EPS)
    strength = jax.nn.sigmoid(pre[:, 0:1])
    rate = misc_ref[3:4, 0:1]
    decay_pre = pre[:, 1:2]
    softplus = jnp.maximum(decay_pre, 0.0) + jnp.log1p(jnp.exp(-jnp.abs(decay_pre)))
    factor = jnp.broadcast_to(jnp.exp(-rate * softplus), (half, size))
    query_t, key_t = query.T, key.T
    match = jnp.sum(query * key, axis=1, keepdims=True)
    readouts = []
    for b in range(half):
        memory = state_ref[b]
        key_col = jnp.broadcast_to(key_t[:, b : b + 1], (size, size))
        query_col = jnp.broadcast_to(query_t[:, b : b + 1], (size, size))
        recalled = jnp.sum(memory * key_col, axis=0, keepdims=True)
        asked = jnp.sum(memory * query_col, axis=0, keepdims=True)
        fade = factor[b : b + 1]
        correction = strength[b : b + 1] * (value[b : b + 1] - fade * recalled)
        updated_ref[b] = fade * memory + key_col * correction
        readouts.append(fade * asked + match[b : b + 1] * correction)
    readout = jnp.concatenate(readouts, axis=0)
    scaling = lax.rsqrt(jnp.mean(readout * readout, axis=1, keepdims=True) + EPS)
    silu = gate / (1.0 + jnp.exp(-gate))
    gated = (scaling * readout * misc_ref[2:3, :] * silu).astype(bf16)
    for z in range(planes):
        spread_ref[z] = gated


def output_kernel(gated_ref, own_ref, other_ref, outs_ref):
    planes, half, size = gated_ref.shape
    my_y = lax.axis_index("y")
    gated = gated_ref[...].reshape(planes * half, size)
    for place, ref in ((my_y, own_ref), (1 - my_y, other_ref)):
        term = dot_t(gated, ref[PARTS]).astype(bf16)
        outs_ref[pl.ds(place * planes, planes)] = term.reshape(planes, half, -1)


def final_kernel(terms_ref, x_ref, updated_ref, out_ref, state_hbm, sem):
    half = terms_ref.shape[1]
    heads = terms_ref.shape[0] // PAIR
    copy = pltpu.make_async_copy(updated_ref, state_hbm, sem)
    copy.start()
    for place in range(PAIR):
        where = slice(place * half, (place + 1) * half)
        total = x_ref[where, :].astype(f32)
        for head in range(heads):
            total = total + terms_ref[place * heads + head].astype(f32)
        out_ref[where, :] = total.astype(bf16)
    copy.wait()


def per_device(
    stream,
    norm_gain,
    query_weight,
    key_weight,
    value_weight,
    gate_weight,
    write_weight,
    decay_weight,
    decay_rate,
    head_gain,
    out_weight,
    state,
):
    planes = lax.axis_size("z")
    heads = lax.axis_size("h")
    rows, cols = stream.shape
    half = rows // PAIR
    size = head_gain.shape[0]
    vmem, anywhere = pl.BlockSpec(memory_space=pltpu.VMEM), pl.BlockSpec(memory_space=pl.ANY)
    kept, plain = pltpu.VMEM, jax.ShapeDtypeStruct

    def call(kernel, outs, *args):
        args = [pltpu.with_memory_space_constraint(arg, pltpu.VMEM) for arg in args]
        specs = jax.tree.map(lambda _: vmem, outs)
        return pl.pallas_call(
            kernel, out_shape=outs, in_specs=[vmem] * len(args), out_specs=specs
        )(*args)

    whole = (norm_gain.reshape(-1, cols), write_weight.T, decay_weight.T)
    whole += (decay_rate.reshape(1, -1), head_gain.reshape(1, -1))
    blocks, own, x, misc = pl.pallas_call(
        stage_kernel,
        out_shape=(
            kept((PAIR * heads, half, cols), bf16),
            kept((PARTS + 1, cols, size), bf16),
            kept((rows, cols), bf16),
            kept((8, cols), f32),
        ),
        in_specs=[anywhere] * 11,
        out_specs=(vmem,) * 4,
        scratch_shapes=[
            pltpu.VMEM(whole[0].shape, bf16),
            pltpu.VMEM((heads, PAIR * cols), bf16),
            pltpu.VMEM((heads, PAIR * cols), bf16),
            pltpu.VMEM(whole[3].shape, f32),
            pltpu.VMEM(whole[4].shape, bf16),
            pltpu.SemaphoreType.DMA((11,)),
        ],
    )(stream, *whole, query_weight, key_weight, value_weight, gate_weight, out_weight)
    other = lax.ppermute(own, "y", [(0, 1), (1, 0)])
    got = lax.all_to_all(blocks, ("y", "h"), 0, 0)
    packed = call(
        project_kernel,
        kept((planes, PARTS * half + half // PAIR, size), bf16),
        got, own, other, misc,
    )
    recv = lax.all_to_all(packed, "z", 0, 0)
    spread, updated = call(
        lambda *refs: state_kernel(cols * PAIR * planes, *refs),
        (kept((planes, half, size), bf16), kept(state.shape, f32)),
        recv, state, misc,
    )
    all_gated = lax.all_to_all(spread, "z", 0, 0)
    outs = call(output_kernel, kept((PAIR * planes, half, cols), bf16), all_gated, own, other)
    terms = lax.all_to_all(outs, ("y", "h"), 0, 0)
    last = [pltpu.with_memory_space_constraint(arg, pltpu.VMEM) for arg in (terms, x, updated)]
    return tuple(
        pl.pallas_call(
            final_kernel,
            out_shape=(plain((rows, cols), bf16), plain(state.shape, f32)),
            in_specs=[vmem] * 3,
            out_specs=(vmem, anywhere),
            scratch_shapes=[pltpu.SemaphoreType.DMA],
        )(*last)
    )


def solution(mesh):
    heads = 16
    grid = Mesh(mesh.devices.reshape(-1, PAIR, heads), ("z", "y", "h"))
    every = ("z", "y", "h")
    flat, cube, same = P(every, None), P(every, None, None), P()
    placed = (flat, same, flat, flat, flat, flat, same, same, same, same, flat, cube)
    return jax.shard_map(
        per_device, mesh=grid, in_specs=placed, out_specs=(flat, cube), check_vma=False
    )
```

time: 101 us -> 89 us (0.88)
  blocking collectives: 16.4 us -> 77.9 us
  starting transfers between devices: 40.3 us -> 5.64 us
  waiting for transfers between devices: 23.2 us -> 0.01 us
  local copies, waits for them, and re-layouts: 12.1 us -> 0.01 us
  other arithmetic: 4.92 us -> 0 us
  Pallas kernels: 0 us -> 4.43 us
  matrix products: 1.81 us -> 0 us
    all_to_all x1 -> x4, blocking collectives: 16.4 us -> 77.9 us  [the longest x1 26.9 us: per_device(): recv = lax.all_to_all(packed, 'z', 0, 0)]
    all_to_all x3 -> x0, starting transfers between devices: 35.4 us -> none  [the longest x1 13 us: per_device(): summed = lax.all_to_all(packed, 'z', 0, 0).astype(f32).sum(axis=0)]
    all_to_all x3 -> x0, waiting for transfers between devices: 23.2 us -> none  [the longest x1 11.6 us: per_device(): summed = lax.all_to_all(packed, 'z', 0, 0).astype(f32).sum(axis=0)]
    unnamed x31 -> x2, local copies, waits for them, and re-layouts: 7.84 us -> 0.01 us
    pallas_call x0 -> x5, Pallas kernels: none -> 4.43 us  [the longest x3 1.75 us: call(): pl.pallas_call(kernel, out_shape=outs, in_specs=[vmem] * len(args), out_s...]
    reduce_sum x8 -> x0, other arithmetic: 2.42 us -> none  [the longest x1 1.53 us: per_device(): readout = jnp.sum(updated * query_vec[:, :, None], axis=1)]
    broadcast_in_dim x2 -> x0, local copies, waits for them, and re-layouts: 2.01 us -> none  [the longest x1 1.37 us: per_device(): jnp.broadcast_to(stream.reshape(PAIR, 1, half, cols), (PAIR, heads, half,...]
    convert_element_type x6 -> x0, other arithmetic: 1.88 us -> none  [the longest x1 0.84 us: gained_of(): gain = lax.dynamic_slice_in_dim(norm_gain, start, cols, 0).astype(f32)]
  transfers between devices with their start and end apart: 4 -> 1, of which waited for: 2 -> 0; matrix products, arithmetic and copies ran while one was open for 4% -> 0% of each run, Pallas kernels for 0% -> 0%
where the time goes in v2:
time: 89 us; the launch traced here: 88.7 us
  blocking collectives  77.9 us (88%)
  starting transfers between devices  5.64 us (6%)
  Pallas kernels  4.43 us (5%)
    all_to_all x1, blocking collectives, per_device(): recv = lax.all_to_all(packed, 'z', 0, 0)  26.9 us
    all_to_all x1, blocking collectives, per_device(): all_gated = lax.all_to_all(spread, 'z', 0, 0)  22.6 us
    all_to_all x1, blocking collectives, per_device(): got = lax.all_to_all(blocks, ('y', 'h'), 0, 0)  15.5 us
    all_to_all x1, blocking collectives, per_device(): terms = lax.all_to_all(outs, ('y', 'h'), 0, 0)  12.9 us
    ppermute x1, starting transfers between devices, per_device(): other = lax.ppermute(own, 'y', [(0, 1), (1, 0)])  5.64 us
  transfers between devices with their start and end apart: 1, of which 0 were waited for; matrix products, arithmetic and copies ran while one was open for 0% of the time, Pallas kernels for 0%

profile of v2, /device:TPU:1, one launch (start us, length us, event | category | flops | bytes accessed | tf_op | source)
XLA Modules:
  0.0 88.7 jit_solution(10848015480789216089)
XLA Ops:
  0.6 0.0 copy-start
  0.6 1.1 %shard_map.131 = (bf16[32,16,128]{2,1,0:T(8,128)(2,1)S(1)}, bf16[5,128,128]{2,1,0:T(8,128)(2,1)S(1)}, bf16[32,128]{1,0:T(8,128)(2,1)S(1)}, f32[8,128]{1,0:T(8,128)S(1)}) custom-call(bf16[32,128]{1,0:T(8,128)(2,1)} %x_hbm.1, bf16[32,128]{1,0:T(8,128)(2,1)} %bitcast.7, bf16[16,4096]{1,0:T(8,128)(2,1)} %bitcast.5, bf16[16,4096]{1,0:T(8,128)(2,1)} %bitcast.6, ...), custom_call_target="tpu_custom_call" | custom-call | tf_op jit(solution)/shard_map/pallas_call | solution.py:191
  1.8 5.6 %collective-permute-start = (bf16[5,128,128]{2,1,0:T(8,128)(2,1)S(1)}, bf16[5,128,128]{2,1,0:T(8,128)(2,1)S(1)}, u32[]{:S(2)}, u32[]{:S(2)}) collective-permute-start(bf16[5,128,128]{2,1,0:T(8,128)(2,1)S(1)} %get-tuple-element.9.own_ref), channel_id=1, source_target_pairs={{0,16},{16,0},{1,17},{17,1},{2,18},{18,2},{3,19},{19,3},{4,20},{20... | collective-permute-start | bytes 491528 | tf_op jit(solution)/shard_map/ppermute | solution.py:210
  7.4 15.5 %all_to_all.20.got_ref = bf16[32,16,128]{2,1,0:T(8,128)(2,1)S(1)} all-to-all(bf16[32,16,128]{2,1,0:T(8,128)(2,1)S(1)} %get-tuple-element.8), channel_id=1, replica_groups=mesh['z'=16,'y'=2,'h'=16] {'y','h'}, dimensions={0} | all-to-all | bytes 262144 | tf_op jit(solution)/shard_map/all_to_all | solution.py:211
  22.9 0.0 collective-permute-done.other_ref
  22.9 0.3 shard_map.132
  23.2 26.9 %all_to_all.21.refs_0_ = bf16[16,72,128]{2,1,0:T(8,128)(2,1)S(1)} all-to-all(bf16[16,72,128]{2,1,0:T(8,128)(2,1)S(1)} %shard_map.132), channel_id=1, replica_groups=mesh['z'=16,'y'=2,'h'=16] {'z'}, dimensions={0} | all-to-all | bytes 589824 | tf_op jit(solution)/shard_map/all_to_all | solution.py:217
  50.1 0.0 copy-done
  50.1 1.2 %shard_map.133 = (bf16[16,16,128]{2,1,0:T(8,128)(2,1)S(1)}, f32[16,128,128]{2,1,0:T(8,128)S(1)}) custom-call(bf16[16,72,128]{2,1,0:T(8,128)(2,1)S(1)} %all_to_all.21.refs_0_, f32[16,128,128]{2,1,0:T(8,128)S(1)} %copy-done, f32[8,128]{1,0:T(8,128)S(1)} %get-tuple-element.10.misc_ref.refs_2_), custom_call_target="tpu_custom_call" | custom-call | tf_op jit(solution)/shard_map/pallas_call | solution.py:185
  51.4 22.6 %all_to_all.22.gated_ref = bf16[16,16,128]{2,1,0:T(8,128)(2,1)S(1)} all-to-all(bf16[16,16,128]{2,1,0:T(8,128)(2,1)S(1)} %get-tuple-element.11), channel_id=1, replica_groups=mesh['z'=16,'y'=2,'h'=16] {'z'}, dimensions={0} | all-to-all | bytes 131072 | tf_op jit(solution)/shard_map/all_to_all | solution.py:223
  74.0 0.2 shard_map.134
  74.2 12.9 %all_to_all.23.terms_ref = bf16[32,16,128]{2,1,0:T(8,128)(2,1)S(1)} all-to-all(bf16[32,16,128]{2,1,0:T(8,128)(2,1)S(1)} %shard_map.134), channel_id=1, replica_groups=mesh['z'=16,'y'=2,'h'=16] {'y','h'}, dimensions={0} | all-to-all | bytes 262144 | tf_op jit(solution)/shard_map/all_to_all | solution.py:225
  87.1 1.6 %shard_map.135 = (bf16[32,128]{1,0:T(8,128)(2,1)}, f32[16,128,128]{2,1,0:T(8,128)}) custom-call(bf16[32,16,128]{2,1,0:T(8,128)(2,1)S(1)} %all_to_all.23.terms_ref, bf16[32,128]{1,0:T(8,128)(2,1)S(1)} %get-tuple-element.12.x_ref, f32[16,128,128]{2,1,0:T(8,128)S(1)} %get-tuple-element.13.updated_ref), custom_call_target="tpu_custom_call" | custom-call | tf_op jit(solution)/shard_map/pallas_call | solution.py:228
Async XLA Ops:
  0.6 49.5 %copy-start = (f32[16,128,128]{2,1,0:T(8,128)S(1)}, f32[16,128,128]{2,1,0:T(8,128)}, u32[]{:S(2)}) copy-start(f32[16,128,128]{2,1,0:T(8,128)} %refs_1_.3) | copy-start | bytes 3145732
  1.8 21.1 %collective-permute-start = (bf16[5,128,128]{2,1,0:T(8,128)(2,1)S(1)}, bf16[5,128,128]{2,1,0:T(8,128)(2,1)S(1)}, u32[]{:S(2)}, u32[]{:S(2)}) collective-permute-start(bf16[5,128,128]{2,1,0:T(8,128)(2,1)S(1)} %get-tuple-element.9.own_ref), channel_id=1, source_target_pairs={{0,16},{16,0},{1,17},{17,1},{2,18},{18,2},{3,19},{19,3},{4,20},{20... | collective-permute-start | bytes 491528 | tf_op jit(solution)/shard_map/ppermute | solution.py:210

commit v3 on v2

v3 whole, which is shorter than its diff:
```python
import jax
import jax.numpy as jnp
from jax import lax
from jax.experimental import pallas as pl
from jax.experimental.pallas import tpu as pltpu
from jax.sharding import Mesh, PartitionSpec as P


EPS = 1e-06
PAIR = 2
PARTS = 4
KEPT = 2
f32, bf16 = jnp.float32, jnp.bfloat16


def row_of(values, index):
    here = lax.broadcasted_iota(jnp.int32, values.shape, 0) == index
    return jnp.sum(jnp.where(here, values, 0.0), axis=0, keepdims=True)


def dot_t(a, b):
    return lax.dot_general(a, b, (((1,), (1,)), ((), ())), preferred_element_type=f32)


def stage_kernel(
    x_hbm, gain_hbm, write_hbm, decay_hbm, rate_hbm, head_gain_hbm, *refs
):
    weights, (blocks_hbm, own_ref, x_ref, misc_ref), scratch = refs[:5], refs[5:9], refs[9:]
    half_ref, gain_ref, write_ref, decay_ref, rate_ref, head_gain_ref, sems = scratch
    half = blocks_hbm.shape[1]
    heads = blocks_hbm.shape[0] // (2 * PAIR)
    cols = blocks_hbm.shape[2]
    my_zh, my_za = lax.axis_index("zh"), lax.axis_index("za")
    my_z, my_y, my_h = my_zh * 2 + my_za, lax.axis_index("y"), lax.axis_index("h")
    here = pl.ds(pl.multiple_of(my_z * (PAIR * cols), PAIR * cols), PAIR * cols)
    moves = [(x_hbm, x_ref)] + [(ref, own_ref.at[m]) for m, ref in enumerate(weights)]
    moves += [
        (gain_hbm, gain_ref),
        (write_hbm.at[:, here], write_ref),
        (decay_hbm.at[:, here], decay_ref),
        (rate_hbm, rate_ref),
        (head_gain_hbm, head_gain_ref),
    ]
    copies = [pltpu.make_async_copy(a, b, sems.at[i]) for i, (a, b) in enumerate(moves)]
    for copy in copies:
        copy.start()
    copies[0].wait()
    for place in range(PAIR):
        rows = x_ref[place * half : (place + 1) * half, :]
        for head in range(heads):
            half_ref[place * heads + head] = rows
    spreads = [
        pltpu.make_async_copy(
            half_ref,
            blocks_hbm.at[pl.ds(plane * PAIR * heads, PAIR * heads)],
            sems.at[len(moves) + plane],
        )
        for plane in range(2)
    ]
    for copy in spreads:
        copy.start()
    for copy in copies[1:]:
        copy.wait()
    gains = gain_ref[...].astype(f32)
    lines = [
        row_of(gains, (my_zh * 2 + plane) * PAIR + place)
        for plane in (my_za, 1 - my_za)
        for place in (my_y, 1 - my_y)
    ]
    lines.append(head_gain_ref[...].astype(f32))
    rates = rate_ref[...]
    lane = lax.broadcasted_iota(jnp.int32, rates.shape, 1)
    rate = jnp.sum(jnp.where(lane == my_h, rates, 0.0), axis=1, keepdims=True)
    lines.append(jnp.broadcast_to(rate, (1, cols)))
    for ref in (write_ref, decay_ref):
        row = row_of(ref[...].astype(f32), my_h)
        low, high = row[:, :cols], row[:, cols:]
        lines.append(jnp.where(my_y == 0, low, high))
        lines.append(jnp.where(my_y == 0, high, low))
    for i, line in enumerate(lines):
        misc_ref[i : i + 1, :] = line
    for copy in spreads:
        copy.wait()


def send_kernel(own_ref, other_ref, far_ref):
    theirs = (1 - lax.axis_index("za")) * KEPT
    for i, ref in enumerate((own_ref, other_ref)):
        for m in range(KEPT):
            far_ref[i * KEPT + m] = ref[theirs + m]


def load_kernel(state_hbm, state_ref, sem):
    copy = pltpu.make_async_copy(state_hbm, state_ref, sem)
    copy.start()
    copy.wait()


def project_kernel(got_ref, own_ref, other_ref, far_ref, misc_ref, packed_ref):
    planes, half = packed_ref.shape[0], got_ref.shape[1]
    cols = got_ref.shape[2]
    heads = got_ref.shape[0] // (2 * PAIR)
    seqs = heads * half
    my_za, my_y = lax.axis_index("za"), lax.axis_index("y")
    squares, gained, small = None, [], None
    for p, plane in enumerate((my_za, 1 - my_za)):
        for i, place in enumerate((my_y, 1 - my_y)):
            x = got_ref[pl.ds((plane * PAIR + place) * heads, heads)]
            x = x.reshape(seqs, cols).astype(f32)
            line = p * PAIR + i
            g = (x * misc_ref[line : line + 1, :]).astype(bf16)
            gained.append(g)
            if p:
                continue
            squares = x * x if squares is None else squares + x * x
            line = lax.broadcasted_iota(jnp.int32, (128, cols), 0)
            write_row, decay_row = misc_ref[6 + i : 7 + i, :], misc_ref[8 + i : 9 + i, :]
            rows = jnp.where(line == 0, write_row, jnp.where(line == 1, decay_row, 0.0))
            term = dot_t(g, rows.astype(bf16))
            small = term if small is None else small + term
    for m in range(KEPT):
        mine = my_za * KEPT + m
        weights = (own_ref[mine], other_ref[mine], far_ref[m], far_ref[KEPT + m])
        part = None
        for g, weight in zip(gained, weights):
            term = jnp.dot(g, weight, preferred_element_type=f32)
            part = term if part is None else part + term
        packed_ref[:, m * half : (m + 1) * half, :] = part.astype(bf16).reshape(planes, half, -1)
    total = jnp.sum(squares, axis=1, keepdims=True)
    lane = lax.broadcasted_iota(jnp.int32, small.shape, 1)
    small = jnp.where(lane == 2, total, small).reshape(planes, PAIR, half // PAIR, 128)
    tail = small[:, 0] + pltpu.roll(small[:, 1].reshape(-1, 128), 64, 1).reshape(planes, -1, 128)
    packed_ref[:, KEPT * half :, :] = tail.astype(bf16)


def state_kernel(width, recv_ref, state_ref, misc_ref, spread_ref, updated_ref):
    planes, half, size = spread_ref.shape
    sums = [recv_ref[0].astype(f32), recv_ref[1].astype(f32)]
    for z in range(2, planes):
        sums[z % 2] = sums[z % 2] + recv_ref[z].astype(f32)
    tail = sums[0][KEPT * half :] + sums[1][KEPT * half :]
    tail = jnp.concatenate([tail, pltpu.roll(tail, 64, 1)], axis=0)
    row_scale = lax.rsqrt(tail[:, 2:3] / width + EPS)

    def scaled(value):
        return (value * row_scale).astype(bf16).astype(f32)

    query, key, value, gate = [
        scaled(sums[p][m * half : (m + 1) * half]) for p in range(2) for m in range(KEPT)
    ]
    pre = scaled(tail)
    query = query * lax.rsqrt(jnp.sum(query * query, axis=1, keepdims=True) + EPS) * size**-0.5
    key = key * lax.rsqrt(jnp.sum(key * key, axis=1, keepdims=True) + EPS)
    strength = jax.nn.sigmoid(pre[:, 0:1])
    rate = misc_ref[5:6, 0:1]
    decay_pre = pre[:, 1:2]
    softplus = jnp.maximum(decay_pre, 0.0) + jnp.log1p(jnp.exp(-jnp.abs(decay_pre)))
    factor = jnp.broadcast_to(jnp.exp(-rate * softplus), (half, size))
    query_t, key_t = query.T, key.T
    match = jnp.sum(query * key, axis=1, keepdims=True)
    recalls, asks = [], []
    for b in range(half):
        memory = state_ref[b]
        key_col = jnp.broadcast_to(key_t[:, b : b + 1], (size, size))
        query_col = jnp.broadcast_to(query_t[:, b : b + 1], (size, size))
        recalls.append(jnp.sum(memory * key_col, axis=0, keepdims=True))
        asks.append(jnp.sum(memory * query_col, axis=0, keepdims=True))
    recalled, asked = jnp.concatenate(recalls, axis=0), jnp.concatenate(asks, axis=0)
    correction = strength * (value - factor * recalled)
    readout = factor * asked + match * correction
    for b in range(half):
        key_col = jnp.broadcast_to(key_t[:, b : b + 1], (size, size))
        updated_ref[b] = factor[b : b + 1] * state_ref[b] + key_col * correction[b : b + 1]
    scaling = lax.rsqrt(jnp.mean(readout * readout, axis=1, keepdims=True) + EPS)
    silu = gate / (1.0 + jnp.exp(-gate))
    gated = (scaling * readout * misc_ref[4:5, :] * silu).astype(bf16)
    for z in range(planes):
        spread_ref[z] = gated


def output_kernel(gated_ref, own_ref, other_ref, outs_ref):
    planes, half, size = gated_ref.shape
    my_y = lax.axis_index("y")
    gated = gated_ref[...].reshape(planes * half, size)
    for place, ref in ((my_y, own_ref), (1 - my_y, other_ref)):
        term = dot_t(gated, ref[PARTS]).astype(bf16)
        outs_ref[pl.ds(place * planes, planes)] = term.reshape(planes, half, -1)


def final_kernel(terms_ref, x_ref, updated_ref, out_hbm, state_hbm, out_ref, sems):
    half = terms_ref.shape[1]
    heads = terms_ref.shape[0] // PAIR
    state_copy = pltpu.make_async_copy(updated_ref, state_hbm, sems.at[0])
    state_copy.start()
    for place in range(PAIR):
        where = slice(place * half, (place + 1) * half)
        total = x_ref[where, :].astype(f32)
        for head in range(heads):
            total = total + terms_ref[place * heads + head].astype(f32)
        out_ref[where, :] = total.astype(bf16)
    out_copy = pltpu.make_async_copy(out_ref, out_hbm, sems.at[1])
    out_copy.start()
    state_copy.wait()
    out_copy.wait()


def per_device(
    stream,
    norm_gain,
    query_weight,
    key_weight,
    value_weight,
    gate_weight,
    write_weight,
    decay_weight,
    decay_rate,
    head_gain,
    out_weight,
    state,
):
    planes = lax.axis_size(("zh", "za"))
    heads = lax.axis_size("h")
    rows, cols = stream.shape
    half = rows // PAIR
    size = head_gain.shape[0]
    vmem, anywhere = pl.BlockSpec(memory_space=pltpu.VMEM), pl.BlockSpec(memory_space=pl.ANY)
    kept, plain = pltpu.VMEM, jax.ShapeDtypeStruct

    def call(kernel, outs, *args):
        args = [pltpu.with_memory_space_constraint(arg, pltpu.VMEM) for arg in args]
        specs = jax.tree.map(lambda _: vmem, outs)
        return pl.pallas_call(
            kernel, out_shape=outs, in_specs=[vmem] * len(args), out_specs=specs
        )(*args)

    whole = (norm_gain.reshape(-1, cols), write_weight.T, decay_weight.T)
    whole += (decay_rate.reshape(1, -1), head_gain.reshape(1, -1))
    blocks, own, x, misc = pl.pallas_call(
        stage_kernel,
        out_shape=(
            plain((2 * PAIR * heads, half, cols), bf16),
            kept((PARTS + 1, cols, size), bf16),
            kept((rows, cols), bf16),
            kept((16, cols), f32),
        ),
        in_specs=[anywhere] * 11,
        out_specs=(anywhere, vmem, vmem, vmem),
        scratch_shapes=[
            pltpu.VMEM((PAIR * heads, half, cols), bf16),
            pltpu.VMEM(whole[0].shape, bf16),
            pltpu.VMEM((heads, PAIR * cols), bf16),
            pltpu.VMEM((heads, PAIR * cols), bf16),
            pltpu.VMEM(whole[3].shape, f32),
            pltpu.VMEM(whole[4].shape, bf16),
            pltpu.SemaphoreType.DMA((13,)),
        ],
    )(stream, *whole, query_weight, key_weight, value_weight, gate_weight, out_weight)
    other = lax.ppermute(own, "y", [(0, 1), (1, 0)])
    far = call(send_kernel, kept((PAIR * KEPT, cols, size), bf16), own, other)
    far = lax.ppermute(far, "za", [(0, 1), (1, 0)])
    memory = pl.pallas_call(
        load_kernel,
        out_shape=kept(state.shape, f32),
        in_specs=[anywhere],
        out_specs=vmem,
        scratch_shapes=[pltpu.SemaphoreType.DMA],
    )(state)
    got = lax.all_to_all(blocks, ("za", "y", "h"), 0, 0)
    packed = call(
        project_kernel,
        kept((planes, KEPT * half + half // PAIR, size), bf16),
        got, own, other, far, misc,
    )
    recv = lax.all_to_all(packed, ("zh", "za"), 0, 0)
    spread, updated = call(
        lambda *refs: state_kernel(cols * PAIR * planes, *refs),
        (kept((planes, half, size), bf16), kept(state.shape, f32)),
        recv, memory, misc,
    )
    all_gated = lax.all_to_all(spread, ("zh", "za"), 0, 0)
    outs = call(output_kernel, kept((PAIR * planes, half, cols), bf16), all_gated, own, other)
    terms = lax.all_to_all(outs, ("y", "h"), 0, 0)
    last = [pltpu.with_memory_space_constraint(arg, pltpu.VMEM) for arg in (terms, x, updated)]
    return tuple(
        pl.pallas_call(
            final_kernel,
            out_shape=(plain((rows, cols), bf16), plain(state.shape, f32)),
            in_specs=[vmem] * 3,
            out_specs=(anywhere, anywhere),
            scratch_shapes=[pltpu.VMEM((rows, cols), bf16), pltpu.SemaphoreType.DMA((2,))],
        )(*last)
    )


def solution(mesh):
    heads = 16
    grid = Mesh(mesh.devices.reshape(-1, 2, PAIR, heads), ("zh", "za", "y", "h"))
    every = ("zh", "za", "y", "h")
    flat, cube, same = P(every, None), P(every, None, None), P()
    placed = (flat, same, flat, flat, flat, flat, same, same, same, same, flat, cube)
    return jax.shard_map(
        per_device, mesh=grid, in_specs=placed, out_specs=(flat, cube), check_vma=False
    )
```

time: 89 us -> 93.1 us (1.046)
  blocking collectives: 77.9 us -> 32.7 us
  starting transfers between devices: 5.64 us -> 32.4 us
  waiting for transfers between devices: 0.01 us -> 20.7 us
  Pallas kernels: 4.43 us -> 6.21 us
    all_to_all x3 -> x1, blocking collectives: 65 us -> 18 us  [per_device(): all_gated = lax.all_to_all(spread, ('zh', 'za'), 0, 0)]
    all_to_all x0 -> x2, starting transfers between devices: none -> 24.4 us  [the longest x1 13.5 us: per_device(): recv = lax.all_to_all(packed, ('zh', 'za'), 0, 0)]
    all_to_all x0 -> x2, waiting for transfers between devices: none -> 10.9 us  [the longest x1 10.9 us: per_device(): recv = lax.all_to_all(packed, ('zh', 'za'), 0, 0)]
    ppermute x1, waiting for transfers between devices: 0.01 us -> 6.66 us  [per_device(): other = lax.ppermute(own, 'y', [(0, 1), (1, 0)])]
    ppermute x0 -> x1, waiting for transfers between devices: none -> 3.09 us  [per_device(): far = lax.ppermute(far, 'za', [(0, 1), (1, 0)])]
    ppermute x0 -> x1, starting transfers between devices: none -> 3.06 us  [per_device(): far = lax.ppermute(far, 'za', [(0, 1), (1, 0)])]
    all_to_all x1, blocking collectives: 12.9 us -> 14.7 us  [per_device(): terms = lax.all_to_all(outs, ('y', 'h'), 0, 0)]
    pallas_call x1 -> x2, Pallas kernels: 1.11 us -> 2.76 us  [the longest x1 1.53 us: per_device(): pl.pallas_call(stage_kernel, out_shape=(plain((2 * PAIR * heads, half, co...]
  transfers between devices with their start and end apart: 1 -> 4, of which waited for: 0 -> 3; matrix products, arithmetic and copies ran while one was open for 0% -> 0% of each run, Pallas kernels for 0% -> 1%
where the time goes in v3:
time: 93.1 us; the launch traced here: 92.6 us
  blocking collectives  32.7 us (35%)
  starting transfers between devices  32.4 us (35%)
  waiting for transfers between devices  20.7 us (22%)
  Pallas kernels  6.21 us (7%)
    all_to_all x1, blocking collectives, per_device(): all_gated = lax.all_to_all(spread, ('zh', 'za'), 0, 0)  18 us
    all_to_all x1, blocking collectives, per_device(): terms = lax.all_to_all(outs, ('y', 'h'), 0, 0)  14.7 us
    all_to_all x1, starting transfers between devices, per_device(): recv = lax.all_to_all(packed, ('zh', 'za'), 0, 0)  13.5 us
    all_to_all x1, starting transfers between devices, per_device(): got = lax.all_to_all(blocks, ('za', 'y', 'h'), 0, 0)  10.9 us
    all_to_all x1, waiting for transfers between devices, per_device(): recv = lax.all_to_all(packed, ('zh', 'za'), 0, 0)  10.9 us
    ppermute x1, waiting for transfers between devices, per_device(): other = lax.ppermute(own, 'y', [(0, 1), (1, 0)])  6.66 us
    ppermute x1, starting transfers between devices, per_device(): other = lax.ppermute(own, 'y', [(0, 1), (1, 0)])  4.87 us
    ppermute x1, waiting for transfers between devices, per_device(): far = lax.ppermute(far, 'za', [(0, 1), (1, 0)])  3.09 us
  transfers between devices with their start and end apart: 4, of which 3 were waited for; matrix products, arithmetic and copies ran while one was open for 0% of the time, Pallas kernels for 1%

profile of v3, /device:TPU:1, one launch (start us, length us, event | category | flops | bytes accessed | tf_op | source)
XLA Modules:
  0.0 92.6 jit_solution(13993481992265832655)
XLA Ops:
  0.6 1.5 %shard_map.131 = (bf16[64,16,128]{2,1,0:T(8,128)(2,1)}, bf16[5,128,128]{2,1,0:T(8,128)(2,1)S(1)}, bf16[32,128]{1,0:T(8,128)(2,1)S(1)}, f32[16,128]{1,0:T(8,128)S(1)}) custom-call(bf16[32,128]{1,0:T(8,128)(2,1)} %x_hbm.1, bf16[32,128]{1,0:T(8,128)(2,1)} %bitcast.7, bf16[16,4096]{1,0:T(8,128)(2,1)} %bitcast.5, bf16[16,4096]{1,0:T(8,128)(2,1)} %bitcast.6, ...), custom_call_target="tpu_custom_call" | custom-call | tf_op jit(solution)/shard_map/pallas_call | solution.py:238
  2.2 10.9 %all-to-all-start = ((bf16[64,16,128]{2,1,0:T(8,128)(2,1)}), bf16[64,16,128]{2,1,0:T(8,128)(2,1)S(1)}, u32[]{:S(2)}, u32[]{:S(2)}) async-start(bf16[64,16,128]{2,1,0:T(8,128)(2,1)} %get-tuple-element.8), calls=%async_computation | async-start | bytes 524288 | tf_op jit(solution)/shard_map/all_to_all | solution.py:268
  13.1 4.9 %collective-permute-start = (bf16[5,128,128]{2,1,0:T(8,128)(2,1)S(1)}, bf16[5,128,128]{2,1,0:T(8,128)(2,1)S(1)}, u32[]{:S(2)}, u32[]{:S(2)}) collective-permute-start(bf16[5,128,128]{2,1,0:T(8,128)(2,1)S(1)} %get-tuple-element.9.own_ref), channel_id=1, source_target_pairs={{0,16},{16,0},{1,17},{17,1},{2,18},{18,2},{3,19},{19,3},{4,20},{20... | collective-permute-start | bytes 491528 | tf_op jit(solution)/shard_map/ppermute | solution.py:258
  18.0 6.7 %collective-permute-done.other_ref = bf16[5,128,128]{2,1,0:T(8,128)(2,1)S(1)} collective-permute-done((bf16[5,128,128]{2,1,0:T(8,128)(2,1)S(1)}, bf16[5,128,128]{2,1,0:T(8,128)(2,1)S(1)}, u32[]{:S(2)}, u32[]{:S(2)}) %collective-permute-start) | collective-permute-done | bytes 163872 | tf_op jit(solution)/shard_map/ppermute | solution.py:258
  24.6 3.1 %collective-permute-start.1 = (bf16[4,128,128]{2,1,0:T(8,128)(2,1)S(1)}, bf16[4,128,128]{2,1,0:T(8,128)(2,1)S(1)}, u32[]{:S(2)}, u32[]{:S(2)}) collective-permute-start(bf16[4,128,128]{2,1,0:T(8,128)(2,1)S(1)} %shard_map.132), channel_id=1, source_target_pairs={{0,32},{32,0},{1,33},{33,1},{2,34},{34,2},{3,35},{35,3},{4,36},{36... | collective-permute-start | bytes 393224 | tf_op jit(solution)/shard_map/ppermute | solution.py:260
  27.7 3.1 %collective-permute-done.1.far_ref = bf16[4,128,128]{2,1,0:T(8,128)(2,1)S(1)} collective-permute-done((bf16[4,128,128]{2,1,0:T(8,128)(2,1)S(1)}, bf16[4,128,128]{2,1,0:T(8,128)(2,1)S(1)}, u32[]{:S(2)}, u32[]{:S(2)}) %collective-permute-start.1) | collective-permute-done | bytes 131104 | tf_op jit(solution)/shard_map/ppermute | solution.py:260
  30.8 0.0 all-to-all-done.got_ref
  30.8 1.0 %shard_map.133 = bf16[16,40,128]{2,1,0:T(8,128)(2,1)} custom-call(bf16[64,16,128]{2,1,0:T(8,128)(2,1)S(1)} %all-to-all-done.got_ref, bf16[5,128,128]{2,1,0:T(8,128)(2,1)S(1)} %get-tuple-element.9.own_ref, bf16[5,128,128]{2,1,0:T(8,128)(2,1)S(1)} %collective-permute-done.other_ref, bf16[4,128,128]{2,1,0:T(8,128)(2,1)S(1)} %collective-permute-done.1.far_ref, ...), custom_call_target="tpu_custom_call" | custom-call | tf_op jit(solution)/shard_map/pallas_call | solution.py:232
  31.8 13.5 %all-to-all-start.1 = ((bf16[16,40,128]{2,1,0:T(8,128)(2,1)}), bf16[16,40,128]{2,1,0:T(8,128)(2,1)S(1)}, u32[]{:S(2)}, u32[]{:S(2)}) async-start(bf16[16,40,128]{2,1,0:T(8,128)(2,1)} %shard_map.133), calls=%async_computation.1 | async-start | bytes 327680 | tf_op jit(solution)/shard_map/all_to_all | solution.py:274
  45.3 1.2 %shard_map.134.refs_1_ = f32[16,128,128]{2,1,0:T(8,128)S(1)} custom-call(f32[16,128,128]{2,1,0:T(8,128)} %state_hbm.1), custom_call_target="tpu_custom_call" | custom-call | tf_op jit(solution)/shard_map/pallas_call | solution.py:261
  46.6 10.9 %all-to-all-done.1.refs_0_ = bf16[16,40,128]{2,1,0:T(8,128)(2,1)S(1)} async-done(((bf16[16,40,128]{2,1,0:T(8,128)(2,1)}), bf16[16,40,128]{2,1,0:T(8,128)(2,1)S(1)}, u32[]{:S(2)}, u32[]{:S(2)}) %all-to-all-start.1) | async-done | bytes 163872 | tf_op jit(solution)/shard_map/all_to_all | solution.py:274
  57.5 1.3 %shard_map.135 = (bf16[16,16,128]{2,1,0:T(8,128)(2,1)S(1)}, f32[16,128,128]{2,1,0:T(8,128)S(1)}) custom-call(bf16[16,40,128]{2,1,0:T(8,128)(2,1)S(1)} %all-to-all-done.1.refs_0_, f32[16,128,128]{2,1,0:T(8,128)S(1)} %shard_map.134.refs_1_, f32[16,128]{1,0:T(8,128)S(1)} %get-tuple-element.10.misc_ref.refs_2_), custom_call_target="tpu_custom_call" | custom-call | tf_op jit(solution)/shard_map/pallas_call | solution.py:232
  58.8 18.0 %all_to_all.20.gated_ref = bf16[16,16,128]{2,1,0:T(8,128)(2,1)S(1)} all-to-all(bf16[16,16,128]{2,1,0:T(8,128)(2,1)S(1)} %get-tuple-element.11), channel_id=1, replica_groups=mesh['zh'=8,'za'=2,'y'=2,'h'=16] {'zh','za'}, dimensions={0} | all-to-all | bytes 131072 | tf_op jit(solution)/shard_map/all_to_all | solution.py:280
  76.8 0.2 shard_map.136
  77.0 14.7 %all_to_all.21.terms_ref = bf16[32,16,128]{2,1,0:T(8,128)(2,1)S(1)} all-to-all(bf16[32,16,128]{2,1,0:T(8,128)(2,1)S(1)} %shard_map.136), channel_id=1, replica_groups=mesh['zh'=8,'za'=2,'y'=2,'h'=16] {'y','h'}, dimensions={0} | all-to-all | bytes 262144 | tf_op jit(solution)/shard_map/all_to_all | solution.py:282
  91.7 1.0 %shard_map.137 = (bf16[32,128]{1,0:T(8,128)(2,1)}, f32[16,128,128]{2,1,0:T(8,128)}) custom-call(bf16[32,16,128]{2,1,0:T(8,128)(2,1)S(1)} %all_to_all.21.terms_ref, bf16[32,128]{1,0:T(8,128)(2,1)S(1)} %get-tuple-element.12.x_ref, f32[16,128,128]{2,1,0:T(8,128)S(1)} %get-tuple-element.13.updated_ref), custom_call_target="tpu_custom_call" | custom-call | tf_op jit(solution)/shard_map/pallas_call | solution.py:285
  (1 shorter events, 0.0 us)
Async XLA Ops:
  2.2 28.6 %all-to-all-start = ((bf16[64,16,128]{2,1,0:T(8,128)(2,1)}), bf16[64,16,128]{2,1,0:T(8,128)(2,1)S(1)}, u32[]{:S(2)}, u32[]{:S(2)}) async-start(bf16[64,16,128]{2,1,0:T(8,128)(2,1)} %get-tuple-element.8), calls=%async_computation | async-start | bytes 524288 | tf_op jit(solution)/shard_map/all_to_all | solution.py:268
  13.1 11.5 %collective-permute-start = (bf16[5,128,128]{2,1,0:T(8,128)(2,1)S(1)}, bf16[5,128,128]{2,1,0:T(8,128)(2,1)S(1)}, u32[]{:S(2)}, u32[]{:S(2)}) collective-permute-start(bf16[5,128,128]{2,1,0:T(8,128)(2,1)S(1)} %get-tuple-element.9.own_ref), channel_id=1, source_target_pairs={{0,16},{16,0},{1,17},{17,1},{2,18},{18,2},{3,19},{19,3},{4,20},{20... | collective-permute-start | bytes 491528 | tf_op jit(solution)/shard_map/ppermute | solution.py:258
  24.6 6.2 %collective-permute-start.1 = (bf16[4,128,128]{2,1,0:T(8,128)(2,1)S(1)}, bf16[4,128,128]{2,1,0:T(8,128)(2,1)S(1)}, u32[]{:S(2)}, u32[]{:S(2)}) collective-permute-start(bf16[4,128,128]{2,1,0:T(8,128)(2,1)S(1)} %shard_map.132), channel_id=1, source_target_pairs={{0,32},{32,0},{1,33},{33,1},{2,34},{34,2},{3,35},{35,3},{4,36},{36... | collective-permute-start | bytes 393224 | tf_op jit(solution)/shard_map/ppermute | solution.py:260
  31.8 25.7 %all-to-all-start.1 = ((bf16[16,40,128]{2,1,0:T(8,128)(2,1)}), bf16[16,40,128]{2,1,0:T(8,128)(2,1)S(1)}, u32[]{:S(2)}, u32[]{:S(2)}) async-start(bf16[16,40,128]{2,1,0:T(8,128)(2,1)} %shard_map.133), calls=%async_computation.1 | async-start | bytes 327680 | tf_op jit(solution)/shard_map/all_to_all | solution.py:274

commit v4 on v3

--- a/solution.py
+++ b/solution.py
@@ -125,12 +125,19 @@
         for g, weight in zip(gained, weights):
             term = jnp.dot(g, weight, preferred_element_type=f32)
             part = term if part is None else part + term
-        packed_ref[:, m * half : (m + 1) * half, :] = part.astype(bf16).reshape(planes, half, -1)
+        part = part.astype(bf16).reshape(planes, half // 2, 2, 128)
+        packed_ref[:, m * half // 2 : (m + 1) * half // 2] = part
     total = jnp.sum(squares, axis=1, keepdims=True)
     lane = lax.broadcasted_iota(jnp.int32, small.shape, 1)
-    small = jnp.where(lane == 2, total, small).reshape(planes, PAIR, half // PAIR, 128)
-    tail = small[:, 0] + pltpu.roll(small[:, 1].reshape(-1, 128), 64, 1).reshape(planes, -1, 128)
-    packed_ref[:, KEPT * half :, :] = tail.astype(bf16)
+    small = jnp.where(lane == 2, total, small).T[:8]
+    lane = lax.broadcasted_iota(jnp.int32, (1, 128), 1)
+    for z in range(planes):
+        start = z * half // 128 * 128
+        line = small[:, start : start + 128]
+        mine = lane // half == z % (128 // half)
+        first = jnp.where(mine, line[0:1], pltpu.roll(line[1:2], 64, 1))
+        tail = jnp.concatenate([first, line[2:3]], axis=0)
+        packed_ref[z, KEPT * half // 2] = tail.astype(bf16)
 
 
 def state_kernel(width, recv_ref, state_ref, misc_ref, spread_ref, updated_ref):
@@ -138,9 +145,13 @@
     sums = [recv_ref[0].astype(f32), recv_ref[1].astype(f32)]
     for z in range(2, planes):
         sums[z % 2] = sums[z % 2] + recv_ref[z].astype(f32)
-    tail = sums[0][KEPT * half :] + sums[1][KEPT * half :]
-    tail = jnp.concatenate([tail, pltpu.roll(tail, 64, 1)], axis=0)
-    row_scale = lax.rsqrt(tail[:, 2:3] / width + EPS)
+    tail = sums[0][KEPT * half // 2] + sums[1][KEPT * half // 2]
+    my_z = lax.axis_index("zh") * 2 + lax.axis_index("za")
+    tail = jnp.concatenate([tail, jnp.zeros((6, 128), f32)], axis=0)
+    tail = pltpu.roll(tail, (128 - my_z % (128 // half) * half) % 128, 1)
+    tail = jnp.concatenate([tail, pltpu.roll(tail, 64, 1)], axis=0).T[:half]
+    sums = [part[: KEPT * half // 2].reshape(KEPT * half, size) for part in sums]
+    row_scale = lax.rsqrt(tail[:, 1:2] / width + EPS)
 
     def scaled(value):
         return (value * row_scale).astype(bf16).astype(f32)
@@ -153,7 +164,7 @@
     key = key * lax.rsqrt(jnp.sum(key * key, axis=1, keepdims=True) + EPS)
     strength = jax.nn.sigmoid(pre[:, 0:1])
     rate = misc_ref[5:6, 0:1]
-    decay_pre = pre[:, 1:2]
+    decay_pre = pre[:, 8:9]
     softplus = jnp.maximum(decay_pre, 0.0) + jnp.log1p(jnp.exp(-jnp.abs(decay_pre)))
     factor = jnp.broadcast_to(jnp.exp(-rate * softplus), (half, size))
     query_t, key_t = query.T, key.T
@@ -268,7 +279,7 @@
     got = lax.all_to_all(blocks, ("za", "y", "h"), 0, 0)
     packed = call(
         project_kernel,
-        kept((planes, KEPT * half + half // PAIR, size), bf16),
+        kept((planes, KEPT * half // 2 + 1, 2, size), bf16),
         got, own, other, far, misc,
     )
     recv = lax.all_to_all(packed, ("zh", "za"), 0, 0)

time: 93.1 us -> 92.5 us (level)
    all_to_all x1, blocking collectives: 18 us -> 17 us  [per_device(): all_gated = lax.all_to_all(spread, ('zh', 'za'), 0, 0)]
where the time goes in v4:
time: 92.5 us; the launch traced here: 92 us
  starting transfers between devices  32.4 us (35%)
  blocking collectives  31.9 us (34%)
  waiting for transfers between devices  20.6 us (22%)
  Pallas kernels  6.45 us (7%)
    all_to_all x1, blocking collectives, per_device(): all_gated = lax.all_to_all(spread, ('zh', 'za'), 0, 0)  17 us
    all_to_all x1, blocking collectives, per_device(): terms = lax.all_to_all(outs, ('y', 'h'), 0, 0)  14.9 us
    all_to_all x1, starting transfers between devices, per_device(): recv = lax.all_to_all(packed, ('zh', 'za'), 0, 0)  13.5 us
    all_to_all x1, starting transfers between devices, per_device(): got = lax.all_to_all(blocks, ('za', 'y', 'h'), 0, 0)  10.9 us
    all_to_all x1, waiting for transfers between devices, per_device(): recv = lax.all_to_all(packed, ('zh', 'za'), 0, 0)  10.8 us
    ppermute x1, waiting for transfers between devices, per_device(): other = lax.ppermute(own, 'y', [(0, 1), (1, 0)])  6.66 us
    ppermute x1, starting transfers between devices, per_device(): other = lax.ppermute(own, 'y', [(0, 1), (1, 0)])  4.87 us
    ppermute x1, waiting for transfers between devices, per_device(): far = lax.ppermute(far, 'za', [(0, 1), (1, 0)])  3.09 us
  transfers between devices with their start and end apart: 4, of which 3 were waited for; matrix products, arithmetic and copies ran while one was open for 0% of the time, Pallas kernels for 1%

profile of v4, /device:TPU:1, one launch (start us, length us, event | category | flops | bytes accessed | tf_op | source)
XLA Modules:
  0.0 92.0 jit_solution(7013287706911458171)
XLA Ops:
  0.6 1.5 %shard_map.131 = (bf16[64,16,128]{2,1,0:T(8,128)(2,1)}, bf16[5,128,128]{2,1,0:T(8,128)(2,1)S(1)}, bf16[32,128]{1,0:T(8,128)(2,1)S(1)}, f32[16,128]{1,0:T(8,128)S(1)}) custom-call(bf16[32,128]{1,0:T(8,128)(2,1)} %x_hbm.1, bf16[32,128]{1,0:T(8,128)(2,1)} %bitcast.7, bf16[16,4096]{1,0:T(8,128)(2,1)} %bitcast.5, bf16[16,4096]{1,0:T(8,128)(2,1)} %bitcast.6, ...), custom_call_target="tpu_custom_call" | custom-call | tf_op jit(solution)/shard_map/pallas_call | solution.py:249
  2.2 10.9 %all-to-all-start = ((bf16[64,16,128]{2,1,0:T(8,128)(2,1)}), bf16[64,16,128]{2,1,0:T(8,128)(2,1)S(1)}, u32[]{:S(2)}, u32[]{:S(2)}) async-start(bf16[64,16,128]{2,1,0:T(8,128)(2,1)} %get-tuple-element.8), calls=%async_computation | async-start | bytes 524288 | tf_op jit(solution)/shard_map/all_to_all | solution.py:279
  13.1 4.9 %collective-permute-start = (bf16[5,128,128]{2,1,0:T(8,128)(2,1)S(1)}, bf16[5,128,128]{2,1,0:T(8,128)(2,1)S(1)}, u32[]{:S(2)}, u32[]{:S(2)}) collective-permute-start(bf16[5,128,128]{2,1,0:T(8,128)(2,1)S(1)} %get-tuple-element.9.own_ref), channel_id=1, source_target_pairs={{0,16},{16,0},{1,17},{17,1},{2,18},{18,2},{3,19},{19,3},{4,20},{20... | collective-permute-start | bytes 491528 | tf_op jit(solution)/shard_map/ppermute | solution.py:269
  18.0 6.7 %collective-permute-done.other_ref = bf16[5,128,128]{2,1,0:T(8,128)(2,1)S(1)} collective-permute-done((bf16[5,128,128]{2,1,0:T(8,128)(2,1)S(1)}, bf16[5,128,128]{2,1,0:T(8,128)(2,1)S(1)}, u32[]{:S(2)}, u32[]{:S(2)}) %collective-permute-start) | collective-permute-done | bytes 163872 | tf_op jit(solution)/shard_map/ppermute | solution.py:269
  24.6 3.1 %collective-permute-start.1 = (bf16[4,128,128]{2,1,0:T(8,128)(2,1)S(1)}, bf16[4,128,128]{2,1,0:T(8,128)(2,1)S(1)}, u32[]{:S(2)}, u32[]{:S(2)}) collective-permute-start(bf16[4,128,128]{2,1,0:T(8,128)(2,1)S(1)} %shard_map.132), channel_id=1, source_target_pairs={{0,32},{32,0},{1,33},{33,1},{2,34},{34,2},{3,35},{35,3},{4,36},{36... | collective-permute-start | bytes 393224 | tf_op jit(solution)/shard_map/ppermute | solution.py:271
  27.7 3.1 %collective-permute-done.1.far_ref = bf16[4,128,128]{2,1,0:T(8,128)(2,1)S(1)} collective-permute-done((bf16[4,128,128]{2,1,0:T(8,128)(2,1)S(1)}, bf16[4,128,128]{2,1,0:T(8,128)(2,1)S(1)}, u32[]{:S(2)}, u32[]{:S(2)}) %collective-permute-start.1) | collective-permute-done | bytes 131104 | tf_op jit(solution)/shard_map/ppermute | solution.py:271
  30.8 0.0 all-to-all-done.got_ref
  30.8 1.0 %shard_map.133 = bf16[16,17,2,128]{3,2,1,0:T(2,128)(2,1)} custom-call(bf16[64,16,128]{2,1,0:T(8,128)(2,1)S(1)} %all-to-all-done.got_ref, bf16[5,128,128]{2,1,0:T(8,128)(2,1)S(1)} %get-tuple-element.9.own_ref, bf16[5,128,128]{2,1,0:T(8,128)(2,1)S(1)} %collective-permute-done.other_ref, bf16[4,128,128]{2,1,0:T(8,128)(2,1)S(1)} %collective-permute-done.1.far_ref, ...), custom_call_target="tpu_custom_call" | custom-call | tf_op jit(solution)/shard_map/pallas_call | solution.py:243
  31.8 13.5 %all-to-all-start.1 = ((bf16[16,17,2,128]{3,2,1,0:T(2,128)(2,1)}), bf16[16,17,2,128]{3,2,1,0:T(2,128)(2,1)S(1)}, u32[]{:S(2)}, u32[]{:S(2)}) async-start(bf16[16,17,2,128]{3,2,1,0:T(2,128)(2,1)} %shard_map.133), calls=%async_computation.1 | async-start | bytes 278528 | tf_op jit(solution)/shard_map/all_to_all | solution.py:285
  45.4 1.2 %shard_map.134.refs_1_ = f32[16,128,128]{2,1,0:T(8,128)S(1)} custom-call(f32[16,128,128]{2,1,0:T(8,128)} %state_hbm.1), custom_call_target="tpu_custom_call" | custom-call | tf_op jit(solution)/shard_map/pallas_call | solution.py:272
  46.6 10.8 %all-to-all-done.1.refs_0_ = bf16[16,17,2,128]{3,2,1,0:T(2,128)(2,1)S(1)} async-done(((bf16[16,17,2,128]{3,2,1,0:T(2,128)(2,1)}), bf16[16,17,2,128]{3,2,1,0:T(2,128)(2,1)S(1)}, u32[]{:S(2)}, u32[]{:S(2)}) %all-to-all-start.1) | async-done | bytes 139296 | tf_op jit(solution)/shard_map/all_to_all | solution.py:285
  57.4 1.5 %shard_map.135 = (bf16[16,16,128]{2,1,0:T(8,128)(2,1)S(1)}, f32[16,128,128]{2,1,0:T(8,128)S(1)}) custom-call(bf16[16,17,2,128]{3,2,1,0:T(2,128)(2,1)S(1)} %all-to-all-done.1.refs_0_, f32[16,128,128]{2,1,0:T(8,128)S(1)} %shard_map.134.refs_1_, f32[16,128]{1,0:T(8,128)S(1)} %get-tuple-element.10.misc_ref.refs_2_), custom_call_target="tpu_custom_call" | custom-call | tf_op jit(solution)/shard_map/pallas_call | solution.py:243
  58.9 17.0 %all_to_all.20.gated_ref = bf16[16,16,128]{2,1,0:T(8,128)(2,1)S(1)} all-to-all(bf16[16,16,128]{2,1,0:T(8,128)(2,1)S(1)} %get-tuple-element.11), channel_id=1, replica_groups=mesh['zh'=8,'za'=2,'y'=2,'h'=16] {'zh','za'}, dimensions={0} | all-to-all | bytes 131072 | tf_op jit(solution)/shard_map/all_to_all | solution.py:291
  75.9 0.2 shard_map.136
  76.1 14.9 %all_to_all.21.terms_ref = bf16[32,16,128]{2,1,0:T(8,128)(2,1)S(1)} all-to-all(bf16[32,16,128]{2,1,0:T(8,128)(2,1)S(1)} %shard_map.136), channel_id=1, replica_groups=mesh['zh'=8,'za'=2,'y'=2,'h'=16] {'y','h'}, dimensions={0} | all-to-all | bytes 262144 | tf_op jit(solution)/shard_map/all_to_all | solution.py:293
  91.0 1.0 %shard_map.137 = (bf16[32,128]{1,0:T(8,128)(2,1)}, f32[16,128,128]{2,1,0:T(8,128)}) custom-call(bf16[32,16,128]{2,1,0:T(8,128)(2,1)S(1)} %all_to_all.21.terms_ref, bf16[32,128]{1,0:T(8,128)(2,1)S(1)} %get-tuple-element.12.x_ref, f32[16,128,128]{2,1,0:T(8,128)S(1)} %get-tuple-element.13.updated_ref), custom_call_target="tpu_custom_call" | custom-call | tf_op jit(solution)/shard_map/pallas_call | solution.py:296
  (1 shorter events, 0.0 us)
Async XLA Ops:
  2.2 28.6 %all-to-all-start = ((bf16[64,16,128]{2,1,0:T(8,128)(2,1)}), bf16[64,16,128]{2,1,0:T(8,128)(2,1)S(1)}, u32[]{:S(2)}, u32[]{:S(2)}) async-start(bf16[64,16,128]{2,1,0:T(8,128)(2,1)} %get-tuple-element.8), calls=%async_computation | async-start | bytes 524288 | tf_op jit(solution)/shard_map/all_to_all | solution.py:279
  13.1 11.5 %collective-permute-start = (bf16[5,128,128]{2,1,0:T(8,128)(2,1)S(1)}, bf16[5,128,128]{2,1,0:T(8,128)(2,1)S(1)}, u32[]{:S(2)}, u32[]{:S(2)}) collective-permute-start(bf16[5,128,128]{2,1,0:T(8,128)(2,1)S(1)} %get-tuple-element.9.own_ref), channel_id=1, source_target_pairs={{0,16},{16,0},{1,17},{17,1},{2,18},{18,2},{3,19},{19,3},{4,20},{20... | collective-permute-start | bytes 491528 | tf_op jit(solution)/shard_map/ppermute | solution.py:269
  24.6 6.2 %collective-permute-start.1 = (bf16[4,128,128]{2,1,0:T(8,128)(2,1)S(1)}, bf16[4,128,128]{2,1,0:T(8,128)(2,1)S(1)}, u32[]{:S(2)}, u32[]{:S(2)}) collective-permute-start(bf16[4,128,128]{2,1,0:T(8,128)(2,1)S(1)} %shard_map.132), channel_id=1, source_target_pairs={{0,32},{32,0},{1,33},{33,1},{2,34},{34,2},{3,35},{35,3},{4,36},{36... | collective-permute-start | bytes 393224 | tf_op jit(solution)/shard_map/ppermute | solution.py:271
  31.8 25.6 %all-to-all-start.1 = ((bf16[16,17,2,128]{3,2,1,0:T(2,128)(2,1)}), bf16[16,17,2,128]{3,2,1,0:T(2,128)(2,1)S(1)}, u32[]{:S(2)}, u32[]{:S(2)}) async-start(bf16[16,17,2,128]{3,2,1,0:T(2,128)(2,1)} %shard_map.133), calls=%async_computation.1 | async-start | bytes 278528 | tf_op jit(solution)/shard_map/all_to_all | solution.py:285

commit v5 on v4

--- a/solution.py
+++ b/solution.py
@@ -160,28 +160,28 @@
         scaled(sums[p][m * half : (m + 1) * half]) for p in range(2) for m in range(KEPT)
     ]
     pre = scaled(tail)
-    query = query * lax.rsqrt(jnp.sum(query * query, axis=1, keepdims=True) + EPS) * size**-0.5
-    key = key * lax.rsqrt(jnp.sum(key * key, axis=1, keepdims=True) + EPS)
+    query_norm = lax.rsqrt(jnp.sum(query * query, axis=1, keepdims=True) + EPS) * size**-0.5
+    key_norm = lax.rsqrt(jnp.sum(key * key, axis=1, keepdims=True) + EPS)
     strength = jax.nn.sigmoid(pre[:, 0:1])
     rate = misc_ref[5:6, 0:1]
     decay_pre = pre[:, 8:9]
     softplus = jnp.maximum(decay_pre, 0.0) + jnp.log1p(jnp.exp(-jnp.abs(decay_pre)))
     factor = jnp.broadcast_to(jnp.exp(-rate * softplus), (half, size))
-    query_t, key_t = query.T, key.T
-    match = jnp.sum(query * key, axis=1, keepdims=True)
-    recalls, asks = [], []
+    query_t, key_t = query.T.astype(bf16), key.T.astype(bf16)
+    match = jnp.sum(query * key, axis=1, keepdims=True) * query_norm * key_norm
+    readouts = []
     for b in range(half):
         memory = state_ref[b]
-        key_col = jnp.broadcast_to(key_t[:, b : b + 1], (size, size))
-        query_col = jnp.broadcast_to(query_t[:, b : b + 1], (size, size))
-        recalls.append(jnp.sum(memory * key_col, axis=0, keepdims=True))
-        asks.append(jnp.sum(memory * query_col, axis=0, keepdims=True))
-    recalled, asked = jnp.concatenate(recalls, axis=0), jnp.concatenate(asks, axis=0)
-    correction = strength * (value - factor * recalled)
-    readout = factor * asked + match * correction
-    for b in range(half):
-        key_col = jnp.broadcast_to(key_t[:, b : b + 1], (size, size))
-        updated_ref[b] = factor[b : b + 1] * state_ref[b] + key_col * correction[b : b + 1]
+        key_col = jnp.broadcast_to(key_t[:, b : b + 1], (size, size)).astype(f32)
+        query_col = jnp.broadcast_to(query_t[:, b : b + 1], (size, size)).astype(f32)
+        one = slice(b, b + 1)
+        recalled = jnp.sum(memory * key_col, axis=0, keepdims=True) * key_norm[one]
+        asked = jnp.sum(memory * query_col, axis=0, keepdims=True) * query_norm[one]
+        fade = factor[one]
+        correction = strength[one] * (value[one] - fade * recalled)
+        updated_ref[b] = fade * memory + key_col * (key_norm[one] * correction)
+        readouts.append(fade * asked + match[one] * correction)
+    readout = jnp.concatenate(readouts, axis=0)
     scaling = lax.rsqrt(jnp.mean(readout * readout, axis=1, keepdims=True) + EPS)
     silu = gate / (1.0 + jnp.exp(-gate))
     gated = (scaling * readout * misc_ref[4:5, :] * silu).astype(bf16)

time: 92.5 us -> 92.1 us (level)
  no operation moved by 1% of the time
where the time goes in v5:
time: 92.1 us; the launch traced here: 91.6 us
  starting transfers between devices  32.4 us (35%)
  blocking collectives  31.9 us (35%)
  waiting for transfers between devices  20.6 us (22%)
  Pallas kernels  6.07 us (7%)
    all_to_all x1, blocking collectives, per_device(): all_gated = lax.all_to_all(spread, ('zh', 'za'), 0, 0)  17 us
    all_to_all x1, blocking collectives, per_device(): terms = lax.all_to_all(outs, ('y', 'h'), 0, 0)  14.9 us
    all_to_all x1, starting transfers between devices, per_device(): recv = lax.all_to_all(packed, ('zh', 'za'), 0, 0)  13.5 us
    all_to_all x1, starting transfers between devices, per_device(): got = lax.all_to_all(blocks, ('za', 'y', 'h'), 0, 0)  10.9 us
    all_to_all x1, waiting for transfers between devices, per_device(): recv = lax.all_to_all(packed, ('zh', 'za'), 0, 0)  10.8 us
    ppermute x1, waiting for transfers between devices, per_device(): other = lax.ppermute(own, 'y', [(0, 1), (1, 0)])  6.66 us
    ppermute x1, starting transfers between devices, per_device(): other = lax.ppermute(own, 'y', [(0, 1), (1, 0)])  4.87 us
    ppermute x1, waiting for transfers between devices, per_device(): far = lax.ppermute(far, 'za', [(0, 1), (1, 0)])  3.09 us
  transfers between devices with their start and end apart: 4, of which 3 were waited for; matrix products, arithmetic and copies ran while one was open for 0% of the time, Pallas kernels for 1%

profile of v5, /device:TPU:1, one launch (start us, length us, event | category | flops | bytes accessed | tf_op | source)
XLA Modules:
  0.0 91.6 jit_solution(6428844868846348831)
XLA Ops:
  0.6 1.5 %shard_map.131 = (bf16[64,16,128]{2,1,0:T(8,128)(2,1)}, bf16[5,128,128]{2,1,0:T(8,128)(2,1)S(1)}, bf16[32,128]{1,0:T(8,128)(2,1)S(1)}, f32[16,128]{1,0:T(8,128)S(1)}) custom-call(bf16[32,128]{1,0:T(8,128)(2,1)} %x_hbm.1, bf16[32,128]{1,0:T(8,128)(2,1)} %bitcast.7, bf16[16,4096]{1,0:T(8,128)(2,1)} %bitcast.5, bf16[16,4096]{1,0:T(8,128)(2,1)} %bitcast.6, ...), custom_call_target="tpu_custom_call" | custom-call | tf_op jit(solution)/shard_map/pallas_call | solution.py:249
  2.2 10.9 %all-to-all-start = ((bf16[64,16,128]{2,1,0:T(8,128)(2,1)}), bf16[64,16,128]{2,1,0:T(8,128)(2,1)S(1)}, u32[]{:S(2)}, u32[]{:S(2)}) async-start(bf16[64,16,128]{2,1,0:T(8,128)(2,1)} %get-tuple-element.8), calls=%async_computation | async-start | bytes 524288 | tf_op jit(solution)/shard_map/all_to_all | solution.py:279
  13.1 4.9 %collective-permute-start = (bf16[5,128,128]{2,1,0:T(8,128)(2,1)S(1)}, bf16[5,128,128]{2,1,0:T(8,128)(2,1)S(1)}, u32[]{:S(2)}, u32[]{:S(2)}) collective-permute-start(bf16[5,128,128]{2,1,0:T(8,128)(2,1)S(1)} %get-tuple-element.9.own_ref), channel_id=1, source_target_pairs={{0,16},{16,0},{1,17},{17,1},{2,18},{18,2},{3,19},{19,3},{4,20},{20... | collective-permute-start | bytes 491528 | tf_op jit(solution)/shard_map/ppermute | solution.py:269
  18.0 6.7 %collective-permute-done.other_ref = bf16[5,128,128]{2,1,0:T(8,128)(2,1)S(1)} collective-permute-done((bf16[5,128,128]{2,1,0:T(8,128)(2,1)S(1)}, bf16[5,128,128]{2,1,0:T(8,128)(2,1)S(1)}, u32[]{:S(2)}, u32[]{:S(2)}) %collective-permute-start) | collective-permute-done | bytes 163872 | tf_op jit(solution)/shard_map/ppermute | solution.py:269
  24.6 3.1 %collective-permute-start.1 = (bf16[4,128,128]{2,1,0:T(8,128)(2,1)S(1)}, bf16[4,128,128]{2,1,0:T(8,128)(2,1)S(1)}, u32[]{:S(2)}, u32[]{:S(2)}) collective-permute-start(bf16[4,128,128]{2,1,0:T(8,128)(2,1)S(1)} %shard_map.132), channel_id=1, source_target_pairs={{0,32},{32,0},{1,33},{33,1},{2,34},{34,2},{3,35},{35,3},{4,36},{36... | collective-permute-start | bytes 393224 | tf_op jit(solution)/shard_map/ppermute | solution.py:271
  27.7 3.1 %collective-permute-done.1.far_ref = bf16[4,128,128]{2,1,0:T(8,128)(2,1)S(1)} collective-permute-done((bf16[4,128,128]{2,1,0:T(8,128)(2,1)S(1)}, bf16[4,128,128]{2,1,0:T(8,128)(2,1)S(1)}, u32[]{:S(2)}, u32[]{:S(2)}) %collective-permute-start.1) | collective-permute-done | bytes 131104 | tf_op jit(solution)/shard_map/ppermute | solution.py:271
  30.8 0.0 all-to-all-done.got_ref
  30.8 1.0 %shard_map.133 = bf16[16,17,2,128]{3,2,1,0:T(2,128)(2,1)} custom-call(bf16[64,16,128]{2,1,0:T(8,128)(2,1)S(1)} %all-to-all-done.got_ref, bf16[5,128,128]{2,1,0:T(8,128)(2,1)S(1)} %get-tuple-element.9.own_ref, bf16[5,128,128]{2,1,0:T(8,128)(2,1)S(1)} %collective-permute-done.other_ref, bf16[4,128,128]{2,1,0:T(8,128)(2,1)S(1)} %collective-permute-done.1.far_ref, ...), custom_call_target="tpu_custom_call" | custom-call | tf_op jit(solution)/shard_map/pallas_call | solution.py:243
  31.8 13.5 %all-to-all-start.1 = ((bf16[16,17,2,128]{3,2,1,0:T(2,128)(2,1)}), bf16[16,17,2,128]{3,2,1,0:T(2,128)(2,1)S(1)}, u32[]{:S(2)}, u32[]{:S(2)}) async-start(bf16[16,17,2,128]{3,2,1,0:T(2,128)(2,1)} %shard_map.133), calls=%async_computation.1 | async-start | bytes 278528 | tf_op jit(solution)/shard_map/all_to_all | solution.py:285
  45.4 1.2 %shard_map.134.refs_1_ = f32[16,128,128]{2,1,0:T(8,128)S(1)} custom-call(f32[16,128,128]{2,1,0:T(8,128)} %state_hbm.1), custom_call_target="tpu_custom_call" | custom-call | tf_op jit(solution)/shard_map/pallas_call | solution.py:272
  46.6 10.8 %all-to-all-done.1.refs_0_ = bf16[16,17,2,128]{3,2,1,0:T(2,128)(2,1)S(1)} async-done(((bf16[16,17,2,128]{3,2,1,0:T(2,128)(2,1)}), bf16[16,17,2,128]{3,2,1,0:T(2,128)(2,1)S(1)}, u32[]{:S(2)}, u32[]{:S(2)}) %all-to-all-start.1) | async-done | bytes 139296 | tf_op jit(solution)/shard_map/all_to_all | solution.py:285
  57.4 1.1 %shard_map.135 = (bf16[16,16,128]{2,1,0:T(8,128)(2,1)S(1)}, f32[16,128,128]{2,1,0:T(8,128)S(1)}) custom-call(bf16[16,17,2,128]{3,2,1,0:T(2,128)(2,1)S(1)} %all-to-all-done.1.refs_0_, f32[16,128,128]{2,1,0:T(8,128)S(1)} %shard_map.134.refs_1_, f32[16,128]{1,0:T(8,128)S(1)} %get-tuple-element.10.misc_ref.refs_2_), custom_call_target="tpu_custom_call" | custom-call | tf_op jit(solution)/shard_map/pallas_call | solution.py:243
  58.5 17.0 %all_to_all.20.gated_ref = bf16[16,16,128]{2,1,0:T(8,128)(2,1)S(1)} all-to-all(bf16[16,16,128]{2,1,0:T(8,128)(2,1)S(1)} %get-tuple-element.11), channel_id=1, replica_groups=mesh['zh'=8,'za'=2,'y'=2,'h'=16] {'zh','za'}, dimensions={0} | all-to-all | bytes 131072 | tf_op jit(solution)/shard_map/all_to_all | solution.py:291
  75.5 0.2 shard_map.136
  75.7 14.9 %all_to_all.21.terms_ref = bf16[32,16,128]{2,1,0:T(8,128)(2,1)S(1)} all-to-all(bf16[32,16,128]{2,1,0:T(8,128)(2,1)S(1)} %shard_map.136), channel_id=1, replica_groups=mesh['zh'=8,'za'=2,'y'=2,'h'=16] {'y','h'}, dimensions={0} | all-to-all | bytes 262144 | tf_op jit(solution)/shard_map/all_to_all | solution.py:293
  90.6 1.0 %shard_map.137 = (bf16[32,128]{1,0:T(8,128)(2,1)}, f32[16,128,128]{2,1,0:T(8,128)}) custom-call(bf16[32,16,128]{2,1,0:T(8,128)(2,1)S(1)} %all_to_all.21.terms_ref, bf16[32,128]{1,0:T(8,128)(2,1)S(1)} %get-tuple-element.12.x_ref, f32[16,128,128]{2,1,0:T(8,128)S(1)} %get-tuple-element.13.updated_ref), custom_call_target="tpu_custom_call" | custom-call | tf_op jit(solution)/shard_map/pallas_call | solution.py:296
  (1 shorter events, 0.0 us)
Async XLA Ops:
  2.2 28.6 %all-to-all-start = ((bf16[64,16,128]{2,1,0:T(8,128)(2,1)}), bf16[64,16,128]{2,1,0:T(8,128)(2,1)S(1)}, u32[]{:S(2)}, u32[]{:S(2)}) async-start(bf16[64,16,128]{2,1,0:T(8,128)(2,1)} %get-tuple-element.8), calls=%async_computation | async-start | bytes 524288 | tf_op jit(solution)/shard_map/all_to_all | solution.py:279
  13.1 11.5 %collective-permute-start = (bf16[5,128,128]{2,1,0:T(8,128)(2,1)S(1)}, bf16[5,128,128]{2,1,0:T(8,128)(2,1)S(1)}, u32[]{:S(2)}, u32[]{:S(2)}) collective-permute-start(bf16[5,128,128]{2,1,0:T(8,128)(2,1)S(1)} %get-tuple-element.9.own_ref), channel_id=1, source_target_pairs={{0,16},{16,0},{1,17},{17,1},{2,18},{18,2},{3,19},{19,3},{4,20},{20... | collective-permute-start | bytes 491528 | tf_op jit(solution)/shard_map/ppermute | solution.py:269
  24.6 6.2 %collective-permute-start.1 = (bf16[4,128,128]{2,1,0:T(8,128)(2,1)S(1)}, bf16[4,128,128]{2,1,0:T(8,128)(2,1)S(1)}, u32[]{:S(2)}, u32[]{:S(2)}) collective-permute-start(bf16[4,128,128]{2,1,0:T(8,128)(2,1)S(1)} %shard_map.132), channel_id=1, source_target_pairs={{0,32},{32,0},{1,33},{33,1},{2,34},{34,2},{3,35},{35,3},{4,36},{36... | collective-permute-start | bytes 393224 | tf_op jit(solution)/shard_map/ppermute | solution.py:271
  31.8 25.6 %all-to-all-start.1 = ((bf16[16,17,2,128]{3,2,1,0:T(2,128)(2,1)}), bf16[16,17,2,128]{3,2,1,0:T(2,128)(2,1)S(1)}, u32[]{:S(2)}, u32[]{:S(2)}) async-start(bf16[16,17,2,128]{3,2,1,0:T(2,128)(2,1)} %shard_map.133), calls=%async_computation.1 | async-start | bytes 278528 | tf_op jit(solution)/shard_map/all_to_all | solution.py:285

commit v6 on v5

--- a/solution.py
+++ b/solution.py
@@ -118,15 +118,19 @@
             rows = jnp.where(line == 0, write_row, jnp.where(line == 1, decay_row, 0.0))
             term = dot_t(g, rows.astype(bf16))
             small = term if small is None else small + term
+    mine = my_za * KEPT
+
+    def beside(ref, start):
+        return jnp.concatenate([ref[start + m] for m in range(KEPT)], axis=1)
+
+    near = jnp.concatenate([beside(own_ref, mine), beside(other_ref, mine)], axis=0)
+    far = jnp.concatenate([beside(far_ref, 0), beside(far_ref, KEPT)], axis=0)
+    part = jnp.dot(jnp.concatenate(gained[:2], axis=1), near, preferred_element_type=f32)
+    part = part + jnp.dot(jnp.concatenate(gained[2:], axis=1), far, preferred_element_type=f32)
+    part = part.astype(bf16)
     for m in range(KEPT):
-        mine = my_za * KEPT + m
-        weights = (own_ref[mine], other_ref[mine], far_ref[m], far_ref[KEPT + m])
-        part = None
-        for g, weight in zip(gained, weights):
-            term = jnp.dot(g, weight, preferred_element_type=f32)
-            part = term if part is None else part + term
-        part = part.astype(bf16).reshape(planes, half // 2, 2, 128)
-        packed_ref[:, m * half // 2 : (m + 1) * half // 2] = part
+        piece = part[:, m * 128 : (m + 1) * 128].reshape(planes, half // 2, 2, 128)
+        packed_ref[:, m * half // 2 : (m + 1) * half // 2] = piece
     total = jnp.sum(squares, axis=1, keepdims=True)
     lane = lax.broadcasted_iota(jnp.int32, small.shape, 1)
     small = jnp.where(lane == 2, total, small).T[:8]

time: 92.1 us -> 92.1 us (level)
  no operation moved by 1% of the time
where the time goes in v6:
time: 92.1 us; the launch traced here: 91.6 us
  starting transfers between devices  32.4 us (35%)
  blocking collectives  31.9 us (35%)
  waiting for transfers between devices  20.6 us (22%)
  Pallas kernels  6.05 us (7%)
    all_to_all x1, blocking collectives, per_device(): all_gated = lax.all_to_all(spread, ('zh', 'za'), 0, 0)  17 us
    all_to_all x1, blocking collectives, per_device(): terms = lax.all_to_all(outs, ('y', 'h'), 0, 0)  14.9 us
    all_to_all x1, starting transfers between devices, per_device(): recv = lax.all_to_all(packed, ('zh', 'za'), 0, 0)  13.5 us
    all_to_all x1, starting transfers between devices, per_device(): got = lax.all_to_all(blocks, ('za', 'y', 'h'), 0, 0)  10.9 us
    all_to_all x1, waiting for transfers between devices, per_device(): recv = lax.all_to_all(packed, ('zh', 'za'), 0, 0)  10.8 us
    ppermute x1, waiting for transfers between devices, per_device(): other = lax.ppermute(own, 'y', [(0, 1), (1, 0)])  6.66 us
    ppermute x1, starting transfers between devices, per_device(): other = lax.ppermute(own, 'y', [(0, 1), (1, 0)])  4.87 us
    ppermute x1, waiting for transfers between devices, per_device(): far = lax.ppermute(far, 'za', [(0, 1), (1, 0)])  3.09 us
  transfers between devices with their start and end apart: 4, of which 3 were waited for; matrix products, arithmetic and copies ran while one was open for 0% of the time, Pallas kernels for 1%

profile of v6, /device:TPU:1, one launch (start us, length us, event | category | flops | bytes accessed | tf_op | source)
XLA Modules:
  0.0 91.6 jit_solution(16043673579070184765)
XLA Ops:
  0.6 1.5 %shard_map.131 = (bf16[64,16,128]{2,1,0:T(8,128)(2,1)}, bf16[5,128,128]{2,1,0:T(8,128)(2,1)S(1)}, bf16[32,128]{1,0:T(8,128)(2,1)S(1)}, f32[16,128]{1,0:T(8,128)S(1)}) custom-call(bf16[32,128]{1,0:T(8,128)(2,1)} %x_hbm.1, bf16[32,128]{1,0:T(8,128)(2,1)} %bitcast.7, bf16[16,4096]{1,0:T(8,128)(2,1)} %bitcast.5, bf16[16,4096]{1,0:T(8,128)(2,1)} %bitcast.6, ...), custom_call_target="tpu_custom_call" | custom-call | tf_op jit(solution)/shard_map/pallas_call | solution.py:253
  2.2 10.9 %all-to-all-start = ((bf16[64,16,128]{2,1,0:T(8,128)(2,1)}), bf16[64,16,128]{2,1,0:T(8,128)(2,1)S(1)}, u32[]{:S(2)}, u32[]{:S(2)}) async-start(bf16[64,16,128]{2,1,0:T(8,128)(2,1)} %get-tuple-element.8), calls=%async_computation | async-start | bytes 524288 | tf_op jit(solution)/shard_map/all_to_all | solution.py:283
  13.1 4.9 %collective-permute-start = (bf16[5,128,128]{2,1,0:T(8,128)(2,1)S(1)}, bf16[5,128,128]{2,1,0:T(8,128)(2,1)S(1)}, u32[]{:S(2)}, u32[]{:S(2)}) collective-permute-start(bf16[5,128,128]{2,1,0:T(8,128)(2,1)S(1)} %get-tuple-element.9.own_ref), channel_id=1, source_target_pairs={{0,16},{16,0},{1,17},{17,1},{2,18},{18,2},{3,19},{19,3},{4,20},{20... | collective-permute-start | bytes 491528 | tf_op jit(solution)/shard_map/ppermute | solution.py:273
  18.0 6.7 %collective-permute-done.other_ref = bf16[5,128,128]{2,1,0:T(8,128)(2,1)S(1)} collective-permute-done((bf16[5,128,128]{2,1,0:T(8,128)(2,1)S(1)}, bf16[5,128,128]{2,1,0:T(8,128)(2,1)S(1)}, u32[]{:S(2)}, u32[]{:S(2)}) %collective-permute-start) | collective-permute-done | bytes 163872 | tf_op jit(solution)/shard_map/ppermute | solution.py:273
  24.6 3.1 %collective-permute-start.1 = (bf16[4,128,128]{2,1,0:T(8,128)(2,1)S(1)}, bf16[4,128,128]{2,1,0:T(8,128)(2,1)S(1)}, u32[]{:S(2)}, u32[]{:S(2)}) collective-permute-start(bf16[4,128,128]{2,1,0:T(8,128)(2,1)S(1)} %shard_map.132), channel_id=1, source_target_pairs={{0,32},{32,0},{1,33},{33,1},{2,34},{34,2},{3,35},{35,3},{4,36},{36... | collective-permute-start | bytes 393224 | tf_op jit(solution)/shard_map/ppermute | solution.py:275
  27.7 3.1 %collective-permute-done.1.far_ref = bf16[4,128,128]{2,1,0:T(8,128)(2,1)S(1)} collective-permute-done((bf16[4,128,128]{2,1,0:T(8,128)(2,1)S(1)}, bf16[4,128,128]{2,1,0:T(8,128)(2,1)S(1)}, u32[]{:S(2)}, u32[]{:S(2)}) %collective-permute-start.1) | collective-permute-done | bytes 131104 | tf_op jit(solution)/shard_map/ppermute | solution.py:275
  30.8 0.0 all-to-all-done.got_ref
  30.8 1.0 %shard_map.133 = bf16[16,17,2,128]{3,2,1,0:T(2,128)(2,1)} custom-call(bf16[64,16,128]{2,1,0:T(8,128)(2,1)S(1)} %all-to-all-done.got_ref, bf16[5,128,128]{2,1,0:T(8,128)(2,1)S(1)} %get-tuple-element.9.own_ref, bf16[5,128,128]{2,1,0:T(8,128)(2,1)S(1)} %collective-permute-done.other_ref, bf16[4,128,128]{2,1,0:T(8,128)(2,1)S(1)} %collective-permute-done.1.far_ref, ...), custom_call_target="tpu_custom_call" | custom-call | tf_op jit(solution)/shard_map/pallas_call | solution.py:247
  31.8 13.5 %all-to-all-start.1 = ((bf16[16,17,2,128]{3,2,1,0:T(2,128)(2,1)}), bf16[16,17,2,128]{3,2,1,0:T(2,128)(2,1)S(1)}, u32[]{:S(2)}, u32[]{:S(2)}) async-start(bf16[16,17,2,128]{3,2,1,0:T(2,128)(2,1)} %shard_map.133), calls=%async_computation.1 | async-start | bytes 278528 | tf_op jit(solution)/shard_map/all_to_all | solution.py:289
  45.4 1.2 %shard_map.134.refs_1_ = f32[16,128,128]{2,1,0:T(8,128)S(1)} custom-call(f32[16,128,128]{2,1,0:T(8,128)} %state_hbm.1), custom_call_target="tpu_custom_call" | custom-call | tf_op jit(solution)/shard_map/pallas_call | solution.py:276
  46.6 10.8 %all-to-all-done.1.refs_0_ = bf16[16,17,2,128]{3,2,1,0:T(2,128)(2,1)S(1)} async-done(((bf16[16,17,2,128]{3,2,1,0:T(2,128)(2,1)}), bf16[16,17,2,128]{3,2,1,0:T(2,128)(2,1)S(1)}, u32[]{:S(2)}, u32[]{:S(2)}) %all-to-all-start.1) | async-done | bytes 139296 | tf_op jit(solution)/shard_map/all_to_all | solution.py:289
  57.4 1.1 %shard_map.135 = (bf16[16,16,128]{2,1,0:T(8,128)(2,1)S(1)}, f32[16,128,128]{2,1,0:T(8,128)S(1)}) custom-call(bf16[16,17,2,128]{3,2,1,0:T(2,128)(2,1)S(1)} %all-to-all-done.1.refs_0_, f32[16,128,128]{2,1,0:T(8,128)S(1)} %shard_map.134.refs_1_, f32[16,128]{1,0:T(8,128)S(1)} %get-tuple-element.10.misc_ref.refs_2_), custom_call_target="tpu_custom_call" | custom-call | tf_op jit(solution)/shard_map/pallas_call | solution.py:247
  58.5 17.0 %all_to_all.20.gated_ref = bf16[16,16,128]{2,1,0:T(8,128)(2,1)S(1)} all-to-all(bf16[16,16,128]{2,1,0:T(8,128)(2,1)S(1)} %get-tuple-element.11), channel_id=1, replica_groups=mesh['zh'=8,'za'=2,'y'=2,'h'=16] {'zh','za'}, dimensions={0} | all-to-all | bytes 131072 | tf_op jit(solution)/shard_map/all_to_all | solution.py:295
  75.5 0.2 shard_map.136
  75.7 14.9 %all_to_all.21.terms_ref = bf16[32,16,128]{2,1,0:T(8,128)(2,1)S(1)} all-to-all(bf16[32,16,128]{2,1,0:T(8,128)(2,1)S(1)} %shard_map.136), channel_id=1, replica_groups=mesh['zh'=8,'za'=2,'y'=2,'h'=16] {'y','h'}, dimensions={0} | all-to-all | bytes 262144 | tf_op jit(solution)/shard_map/all_to_all | solution.py:297
  90.6 1.0 %shard_map.137 = (bf16[32,128]{1,0:T(8,128)(2,1)}, f32[16,128,128]{2,1,0:T(8,128)}) custom-call(bf16[32,16,128]{2,1,0:T(8,128)(2,1)S(1)} %all_to_all.21.terms_ref, bf16[32,128]{1,0:T(8,128)(2,1)S(1)} %get-tuple-element.12.x_ref, f32[16,128,128]{2,1,0:T(8,128)S(1)} %get-tuple-element.13.updated_ref), custom_call_target="tpu_custom_call" | custom-call | tf_op jit(solution)/shard_map/pallas_call | solution.py:300
  (1 shorter events, 0.0 us)
Async XLA Ops:
  2.2 28.6 %all-to-all-start = ((bf16[64,16,128]{2,1,0:T(8,128)(2,1)}), bf16[64,16,128]{2,1,0:T(8,128)(2,1)S(1)}, u32[]{:S(2)}, u32[]{:S(2)}) async-start(bf16[64,16,128]{2,1,0:T(8,128)(2,1)} %get-tuple-element.8), calls=%async_computation | async-start | bytes 524288 | tf_op jit(solution)/shard_map/all_to_all | solution.py:283
  13.1 11.5 %collective-permute-start = (bf16[5,128,128]{2,1,0:T(8,128)(2,1)S(1)}, bf16[5,128,128]{2,1,0:T(8,128)(2,1)S(1)}, u32[]{:S(2)}, u32[]{:S(2)}) collective-permute-start(bf16[5,128,128]{2,1,0:T(8,128)(2,1)S(1)} %get-tuple-element.9.own_ref), channel_id=1, source_target_pairs={{0,16},{16,0},{1,17},{17,1},{2,18},{18,2},{3,19},{19,3},{4,20},{20... | collective-permute-start | bytes 491528 | tf_op jit(solution)/shard_map/ppermute | solution.py:273
  24.6 6.2 %collective-permute-start.1 = (bf16[4,128,128]{2,1,0:T(8,128)(2,1)S(1)}, bf16[4,128,128]{2,1,0:T(8,128)(2,1)S(1)}, u32[]{:S(2)}, u32[]{:S(2)}) collective-permute-start(bf16[4,128,128]{2,1,0:T(8,128)(2,1)S(1)} %shard_map.132), channel_id=1, source_target_pairs={{0,32},{32,0},{1,33},{33,1},{2,34},{34,2},{3,35},{35,3},{4,36},{36... | collective-permute-start | bytes 393224 | tf_op jit(solution)/shard_map/ppermute | solution.py:275
  31.8 25.6 %all-to-all-start.1 = ((bf16[16,17,2,128]{3,2,1,0:T(2,128)(2,1)}), bf16[16,17,2,128]{3,2,1,0:T(2,128)(2,1)S(1)}, u32[]{:S(2)}, u32[]{:S(2)}) async-start(bf16[16,17,2,128]{3,2,1,0:T(2,128)(2,1)} %shard_map.133), calls=%async_computation.1 | async-start | bytes 278528 | tf_op jit(solution)/shard_map/all_to_all | solution.py:289
